TPU v7x, 512 devices: a whole 4x4x16 slice. The times are simulated.
512 devices in a mesh: dp: 4 (over x), kv: 64 (over z, y), tp: 2 (over core).
Axes of the slice: x: 4, y: 4, z: 16, core: 2. Of those that a mesh axis runs over, the one named last changes fastest.
Arguments:
- stream: bfloat16 [512, 2048], P('dp', ('kv', 'tp')), parts along dimension 0, may hold values from -40 to 40
- old_state: float32 [512, 8, 64, 128], P(('dp', 'kv'), 'tp'), parts along dimension 0, may hold values from -6 to 6
- decay_amounts: float32 [512, 512], P(('dp', 'kv'), 'tp'), parts along dimension 0, may hold values from 0.003 to 1
- first_gain: float32 [2048], replicated, may hold values from 0.1 to 1.9
- first_gate: bfloat16 [2048, 5632], P(None, ('kv', 'tp')), may hold values from -0.125 to 0.125
- first_up: bfloat16 [2048, 5632], P(None, ('kv', 'tp')), may hold values from -0.125 to 0.125
- first_down: bfloat16 [5632, 2048], P(('kv', 'tp')), may hold values from -0.078125 to 0.078125
- mixer_gain: float32 [2048], P('kv'), may hold values from 0.1 to 1.9
- query_weight: bfloat16 [2048, 512], P('kv', 'tp'), may hold values from -0.125 to 0.125
- key_weight: bfloat16 [2048, 512], P('kv', 'tp'), may hold values from -0.125 to 0.125
- decay_weight: bfloat16 [2048, 512], P('kv', 'tp'), may hold values from -0.5 to 0.5
- value_weight: bfloat16 [2048, 1024], P('kv', 'tp'), may hold values from -0.125 to 0.125
- output_gate_weight: bfloat16 [2048, 1024], P('kv', 'tp'), may hold values from -0.125 to 0.125
- head_gain: float32 [1024], P('tp'), may hold values from 0.1 to 1.9
- output_weight: bfloat16 [1024, 2048], P('tp', 'kv'), may hold values from -0.1875 to 0.1875
- second_gain: float32 [2048], replicated, may hold values from 0.1 to 1.9
- second_gate: bfloat16 [2048, 5632], P(None, ('kv', 'tp')), may hold values from -0.125 to 0.125
- second_up: bfloat16 [2048, 5632], P(None, ('kv', 'tp')), may hold values from -0.125 to 0.125
- second_down: bfloat16 [5632, 2048], P(('kv', 'tp')), may hold values from -0.078125 to 0.078125
Outputs:
- mixed_stream: bfloat16 [512, 2048], P('dp', ('kv', 'tp')), parts along dimension 0
- new_state: float32 [512, 8, 64, 128], P(('dp', 'kv'), 'tp'), parts along dimension 0
There are 4 independent parts, one for each index of `dp`. A program takes and returns all parts, laid end to end along the dimension named above; an argument that names none is the same for every part. Nothing has to cross between parts.
All inputs are finite; a program needn't handle non-finite values.
Results may differ from a plain program's by a relative error of at most 0.007.
Values may be sent and summed in bfloat16 or wider, within the bound.
A program may use at most 64 MiB of HBM per device.

v0:
```python
import math

import jax
import jax.numpy as jnp
from jax import lax
from jax.sharding import PartitionSpec as P

D = 2048


EPSILON = 1e-06
GATE_SOFTNESS = 16.0


def cut_along(value, dim, length):
    dims = value.shape
    parts = value.reshape(*dims[:dim], length, dims[dim] // length, *dims[dim + 1 :])
    return jnp.moveaxis(parts, dim, 0)


def summed_on_arrival(value, axis, dim):
    length = lax.axis_size(axis)
    parts = lax.all_to_all(cut_along(value, dim, length), axis, 0, 0, tiled=True)
    return jnp.sum(parts.astype(jnp.float32), axis=0)


def summed_on_arrival_2(value, axis, dim):
    parts = cut_along(value, dim, lax.axis_size(axis))
    arrived = lax.all_to_all(parts, axis, split_axis=0, concat_axis=0, tiled=True)
    return arrived.sum(axis=0)


def copy_for_each(value, axis):
    length = lax.axis_size(axis)
    return lax.all_to_all(
        jnp.broadcast_to(value[None], (length, *value.shape)), axis, 0, 0, tiled=True
    )


def in_order(parts, dim):
    dims = list(parts.shape[1:])
    dims[dim] *= parts.shape[0]
    return jnp.moveaxis(parts, 0, dim).reshape(dims)


def gathered_copies(value, axis, dim):
    parts = copy_for_each(value, axis)
    return in_order(parts, dim)


def in_one_piece(arrays, axis, dim, along):
    widths = [math.prod(a.shape[along:]) for a in arrays]
    both = jnp.concatenate(
        [a.reshape(*a.shape[:along], w) for a, w in zip(arrays, widths)], axis=along
    )
    result = summed_on_arrival_2(both, axis, dim)
    parts = jnp.split(result, [sum(widths[:k]) for k in range(1, len(widths))], axis=along)
    return tuple(
        (b.reshape(*result.shape[:along], *a.shape[along:]) for a, b in zip(arrays, parts))
    )


def half_block(stream, norm_gain, w_gate, w_up, w_down):
    wide = lax.all_gather(stream, ("kv", "tp"), axis=1, tiled=True).astype(jnp.float32)
    scaled = (wide * norm_gain).astype(jnp.bfloat16)
    gate_acc = jnp.dot(scaled, w_gate, preferred_element_type=jnp.float32)
    up_acc = jnp.dot(scaled, w_up, preferred_element_type=jnp.float32)
    square_acc = jnp.sum(wide * wide, axis=1)
    row_scale = lax.rsqrt(square_acc / norm_gain.shape[0] + EPSILON)[:, None]
    hidden = (jax.nn.silu(gate_acc * row_scale) * (up_acc * row_scale)).astype(jnp.bfloat16)
    partial_out = jnp.dot(hidden, w_down, preferred_element_type=jnp.float32)
    paired = summed_on_arrival(partial_out.astype(jnp.bfloat16), "tp", 0)
    blocked = summed_on_arrival_2(paired, "kv", 1)
    summed = lax.all_to_all(blocked, "tp", split_axis=1, concat_axis=0, tiled=True)
    return (stream.astype(jnp.float32) + 0.5 * summed).astype(jnp.bfloat16)


def body(
    stream,
    old_state,
    decay_amounts,
    first_gain,
    first_gate,
    first_up,
    first_down,
    mixer_gain,
    query_weight,
    key_weight,
    decay_weight,
    value_weight,
    output_gate_weight,
    head_gain,
    output_weight,
    second_gain,
    second_gate,
    second_up,
    second_down,
):
    middle = half_block(stream, first_gain, first_gate, first_up, first_down)
    paired_cols = gathered_copies(middle, "tp", 1)
    wide_cols = paired_cols.astype(jnp.float32)
    scaled = (wide_cols * mixer_gain).astype(jnp.bfloat16)
    query_part = jnp.dot(scaled, query_weight, preferred_element_type=jnp.float32)
    key_part = jnp.dot(scaled, key_weight, preferred_element_type=jnp.float32)
    decay_part = jnp.dot(scaled, decay_weight, preferred_element_type=jnp.float32)
    value_part = jnp.dot(scaled, value_weight, preferred_element_type=jnp.float32)
    outgate_part = jnp.dot(scaled, output_gate_weight, preferred_element_type=jnp.float32)
    local_rows = old_state.shape[0]
    local_heads = old_state.shape[1]
    key_dim = old_state.shape[2]
    value_dim = old_state.shape[3]
    query_sum, key_sum, decay_sum, value_sum, outgate_sum, own_squares = in_one_piece(
        (
            query_part,
            key_part,
            decay_part,
            value_part,
            outgate_part,
            jnp.sum(wide_cols * wide_cols, axis=1),
        ),
        "kv",
        0,
        1,
    )
    row_scale = lax.rsqrt(own_squares / D + EPSILON)[:, None]
    query = (query_sum * row_scale * key_dim ** (-0.5)).reshape(local_rows, local_heads, key_dim)
    keys = (key_sum * row_scale).reshape(local_rows, local_heads, key_dim)
    gate_logits = (decay_sum * row_scale).reshape(local_rows, local_heads, key_dim)
    values = (value_sum * row_scale).reshape(local_rows, local_heads, value_dim)
    decay_logarithm = jax.nn.log_sigmoid(gate_logits) / GATE_SOFTNESS - decay_amounts.reshape(
        local_rows, local_heads, key_dim
    )
    new_state = (
        jnp.exp(decay_logarithm)[..., None] * old_state + keys[..., None] * values[:, :, None, :]
    )
    readout = jnp.einsum("bhk,bhkv->bhv", query, new_state, precision=lax.Precision.HIGHEST)
    normed = readout * lax.rsqrt(jnp.mean(readout * readout, axis=-1, keepdims=True) + EPSILON)
    mixed_heads = (
        normed.reshape(local_rows, local_heads * value_dim)
        * head_gain
        * jax.nn.silu(outgate_sum * row_scale)
    ).astype(jnp.bfloat16)
    projected = jnp.dot(
        gathered_copies(mixed_heads, "kv", 0), output_weight, preferred_element_type=jnp.float32
    ).astype(jnp.bfloat16)
    attention_out = summed_on_arrival(
        lax.optimization_barrier(projected).astype(jnp.float32).astype(jnp.bfloat16), "tp", 1
    )
    after = (middle.astype(jnp.float32) + attention_out).astype(jnp.bfloat16)
    mixed_stream = half_block(after, second_gain, second_gate, second_up, second_down)
    return (mixed_stream, new_state)


def solution(mesh):
    in_specs = (
        P("dp", ("kv", "tp")),
        P(("dp", "kv"), "tp", None, None),
        P(("dp", "kv"), "tp"),
        P(),
        P(None, ("kv", "tp")),
        P(None, ("kv", "tp")),
        P(("kv", "tp"), None),
        P("kv"),
        P("kv", "tp"),
        P("kv", "tp"),
        P("kv", "tp"),
        P("kv", "tp"),
        P("kv", "tp"),
        P("tp"),
        P("tp", "kv"),
        P(),
        P(None, ("kv", "tp")),
        P(None, ("kv", "tp")),
        P(("kv", "tp"), None),
    )
    out_specs = (P("dp", ("kv", "tp")), P(("dp", "kv"), "tp", None, None))
    return jax.shard_map(body, mesh=mesh, in_specs=in_specs, out_specs=out_specs, check_vma=False)
```

profile of v0, /device:TPU:6, one launch (start us, length us, event | category | flops | bytes accessed | tf_op | source)
XLA Modules:
  0.0 384.8 jit_solution(13808392015291764144)
XLA Ops:
  0.6 90.2 %all_gather.6 = bf16[128,2048]{0,1:T(8,128)(2,1)S(1)} all-gather(bf16[128,16]{0,1:T(8,128)(2,1)} %param.19), channel_id=1, replica_groups=mesh['dp'=4,'kv'=64,'tp'=2] {'kv','tp'}, dimensions={1}, use_global_device_ids=true | all-gather | bytes 528384 | tf_op jit(solution)/shard_map/all_gather | solution.py:64
  90.8 0.3 fusion.5
  91.1 0.4 copy-done.13
  91.5 0.2 copy-done.18
  91.8 0.5 convolution_multiply_fusion.3
  92.3 0.4 copy-done.3
  92.7 0.8 convolution_convert_fusion.1
  93.5 4.2 %all_to_all.66 = bf16[2,64,2048]{2,1,0:T(8,128)(2,1)S(1)} all-to-all(bf16[2,64,2048]{2,1,0:T(8,128)(2,1)S(1)} %bitcast.78), channel_id=1, replica_groups=mesh['dp'=4,'kv'=64,'tp'=2] {'tp'}, dimensions={0} | all-to-all | bytes 1048576 | tf_op jit(solution)/shard_map/all_to_all | solution.py:23
  97.7 0.3 copy.89
  98.1 0.7 reshape.152
  98.7 42.7 %all_to_all.67 = f32[64,1,2048]{2,1,0:T(1,128)S(1)} all-to-all(f32[64,1,2048]{2,1,0:T(1,128)S(1)} %reshape.152), channel_id=1, replica_groups=mesh['dp'=4,'kv'=64,'tp'=2] {'kv'}, dimensions={0} | all-to-all | bytes 1048576 | tf_op jit(solution)/shard_map/all_to_all | solution.py:29
  141.4 0.5 broadcast.123
  141.9 1.9 reduce.4
  143.8 0.4 reshape.153
  144.4 3.7 all_to_all.68
  148.1 0.7 reduce.5
  149.0 0.6 copy-done.9
  149.6 3.7 all_to_all.69
  153.8 0.5 copy.93
  154.6 0.6 copy-done.10
  155.4 0.5 copy-done.11
  156.1 0.5 copy-done.12
  156.8 0.6 copy-done.6
  157.6 0.5 copy-done.7
  158.4 1.7 copy.94
  160.1 6.0 %all-to-all-start.4 = ((f32[64,2,1793]{2,1,0:T(2,128)}), f32[64,2,1793]{2,1,0:T(2,128)S(1)}, u32[]{:S(2)}, u32[]{:S(2)}) async-start(f32[64,2,1793]{2,1,0:T(2,128)} %copy.94), calls=%async_computation.4 | async-start | bytes 1966080 | tf_op jit(solution)/shard_map/all_to_all | solution.py:29
  166.2 52.7 %all-to-all-done.4 = f32[64,2,1793]{2,1,0:T(2,128)S(1)} async-done(((f32[64,2,1793]{2,1,0:T(2,128)}), f32[64,2,1793]{2,1,0:T(2,128)S(1)}, u32[]{:S(2)}, u32[]{:S(2)}) %all-to-all-start.4) | async-done | bytes 918048 | tf_op jit(solution)/shard_map/all_to_all | solution.py:29
  218.9 0.4 reduce_sum.94
  220.1 0.3 fusion.47
  220.5 0.6 copy-done.16
  221.3 22.9 %all_to_all.70 = bf16[64,2,512]{2,1,0:T(2,128)(2,1)S(1)} all-to-all(bf16[64,2,512]{2,1,0:T(2,128)(2,1)S(1)} %broadcast_in_dim.5), channel_id=1, replica_groups=mesh['dp'=4,'kv'=64,'tp'=2] {'kv'}, dimensions={0} | all-to-all | bytes 262144 | tf_op jit(solution)/shard_map/all_to_all | solution.py:35
  244.3 0.7 copy-done.8
  245.1 3.7 all_to_all.71
  248.9 80.7 %all_gather.7 = bf16[128,2048]{0,1:T(8,128)(2,1)S(1)} all-gather(bf16[128,16]{0,1:T(8,128)(2,1)S(1)} %add_convert_fusion.1), channel_id=1, replica_groups=mesh['dp'=4,'kv'=64,'tp'=2] {'kv','tp'}, dimensions={1}, use_global_device_ids=true | all-gather | bytes 528384 | tf_op jit(solution)/shard_map/all_gather | solution.py:64
  329.6 0.3 fusion.7
  329.9 0.4 copy-done.14
  330.6 0.5 convolution_multiply_fusion.1
  331.0 0.5 copy-done.4
  331.6 0.8 convolution_convert_fusion
  332.4 4.2 %all_to_all.72 = bf16[2,64,2048]{2,1,0:T(8,128)(2,1)S(1)} all-to-all(bf16[2,64,2048]{2,1,0:T(8,128)(2,1)S(1)} %bitcast.79), channel_id=1, replica_groups=mesh['dp'=4,'kv'=64,'tp'=2] {'tp'}, dimensions={0} | all-to-all | bytes 1048576 | tf_op jit(solution)/shard_map/all_to_all | solution.py:23
  336.6 0.3 copy.96
  336.9 0.7 reshape.156
  337.6 39.5 %all_to_all.73 = f32[64,1,2048]{2,1,0:T(1,128)S(1)} all-to-all(f32[64,1,2048]{2,1,0:T(1,128)S(1)} %reshape.156), channel_id=1, replica_groups=mesh['dp'=4,'kv'=64,'tp'=2] {'kv'}, dimensions={0} | all-to-all | bytes 1048576 | tf_op jit(solution)/shard_map/all_to_all | solution.py:29
  377.1 1.9 reduce.6
  379.0 0.4 reshape.157
  379.6 3.7 all_to_all.74
  383.3 0.7 reduce.7
  384.2 0.6 add_convert_fusion
  (77 shorter events, 4.3 us)
Async XLA Ops:
  0.6 91.6 %copy-start = (bf16[44,2048]{1,0:T(8,128)(2,1)S(1)}, bf16[44,2048]{1,0:T(8,128)(2,1)}, u32[]{:S(2)}) copy-start(bf16[44,2048]{1,0:T(8,128)(2,1)} %param.25) | copy-start | bytes 540676
  90.8 0.7 copy-start.13
  90.8 0.9 copy-start.18
  91.8 0.9 copy-start.3
  148.9 0.7 copy-start.9
  153.8 0.7 copy-start.17
  154.5 0.7 copy-start.10
  155.2 0.7 copy-start.11
  155.9 0.7 copy-start.12
  156.6 0.8 copy-start.6
  157.4 0.8 copy-start.7
  160.1 6.0 %copy-start.15 = (f32[2,256]{1,0:T(2,128)S(1)}, f32[2,256]{1,0:T(2,128)}, u32[]{:S(2)}) copy-start(f32[2,256]{1,0:T(2,128)} %param.21) | copy-start | bytes 6148
  160.1 58.8 %all-to-all-start.4 = ((f32[64,2,1793]{2,1,0:T(2,128)}), f32[64,2,1793]{2,1,0:T(2,128)S(1)}, u32[]{:S(2)}, u32[]{:S(2)}) async-start(f32[64,2,1793]{2,1,0:T(2,128)} %copy.94), calls=%async_computation.4 | async-start | bytes 1966080 | tf_op jit(solution)/shard_map/all_to_all | solution.py:29
  166.2 53.7 %copy-start.2 = (f32[2,4,64,128]{3,2,1,0:T(8,128)S(1)}, f32[2,4,64,128]{3,2,1,0:T(8,128)}, u32[]{:S(2)}) copy-start(f32[2,4,64,128]{3,2,1,0:T(8,128)} %param.20) | copy-start | bytes 786436
  220.0 24.2 %copy-start.1 = (f32[2,4,64,128]{3,2,1,0:T(8,128)}, f32[2,4,64,128]{3,2,1,0:T(8,128)S(1)}, u32[]{:S(2)}) copy-start(f32[2,4,64,128]{3,2,1,0:T(8,128)S(1)} %multiply_add_fusion) | copy-start | bytes 786436
  220.5 0.7 copy-start.16
  244.2 0.8 copy-start.8
  329.6 0.7 copy-start.14
  329.6 0.9 copy-start.19
  330.6 0.9 copy-start.4
  330.6 1.0 copy-start.5
where the time goes:
time: 387 us; the launch traced here: 385 us
  blocking collectives  299 us (77%)
  waiting for transfers between devices  52.7 us (14%)
  local copies, waits for them, and re-layouts  14.2 us (4%)
  other arithmetic  7.92 us (2%)
  starting transfers between devices  5.97 us (2%)
    all_gather x2, blocking collectives, half_block(): lax.all_gather(stream, ('kv', 'tp'), axis=1, tiled=True).astype(jnp.float32)  171 us
    all_to_all x2, blocking collectives, summed_on_arrival_2(): lax.all_to_all(parts, axis, split_axis=0, concat_axis=0, tiled=True)  82.2 us
    all_to_all x1, waiting for transfers between devices, summed_on_arrival_2(): lax.all_to_all(parts, axis, split_axis=0, concat_axis=0, tiled=True)  52.7 us
    all_to_all x2, blocking collectives, copy_for_each(): lax.all_to_all(jnp.broadcast_to(value[None], (length, *value.shape)), axi...  26.6 us
    all_to_all x3, blocking collectives, summed_on_arrival(): lax.all_to_all(cut_along(value, dim, length), axis, 0, 0, tiled=True)  12 us
    unnamed x48, local copies, waits for them, and re-layouts  9.67 us
  transfers between devices with their start and end apart: 1, of which 1 were waited for; matrix products, arithmetic and copies ran while one was open for 0% of the time, Pallas kernels for 0%

commit v1 on v0

v1 whole, which is shorter than its diff:
```python
import functools

import jax
import jax.numpy as jnp
from jax import lax
from jax.experimental import pallas as pl
from jax.experimental.pallas import tpu as pltpu
from jax.sharding import PartitionSpec as P

EPSILON = 1e-06
GATE_SOFTNESS = 16.0
NY = 4
C = 16
HID = 48
NF = 15
F32 = jnp.float32
BF16 = jnp.bfloat16


def copy_to(src, dst, send, recv, **where):
    return pltpu.make_async_remote_copy(
        src_ref=src,
        dst_ref=dst,
        send_sem=send,
        recv_sem=recv,
        device_id=where,
        device_id_type=pl.DeviceIdType.MESH,
    )


def dot(a, b, ca, cb):
    return lax.dot_general(a, b, (((ca,), (cb,)), ((), ())), preferred_element_type=F32)


def kernel(
    NZ,
    FFL,
    sT,
    old,
    dec,
    g1,
    wg1,
    wu1,
    wd1,
    gm,
    wq,
    wk,
    wz,
    wv,
    wo,
    hg,
    wout,
    g2,
    wg2,
    wu2,
    wd2,
    outT,
    new,
    gat1,
    gat2,
    wgu1,
    wgu2,
    wdt1,
    wdt2,
    s0,
    psend,
    own,
    ptp,
    ysend,
    yrecv,
    accf,
    zsend,
    zrecv,
    pair,
    psnd,
    prcv,
    zs,
    zsb,
    zrb,
    mg,
    mgf,
    pj,
    pjr,
    aft,
    ag_z,
    ag_y,
    ag_t,
    rs_t,
    rs_y,
    rs_z,
    tp_s,
    pr_y,
    pr_z,
    mh_y,
    mh_z,
    fin_s,
):
    kv = lax.axis_index("kv")
    t = lax.axis_index("tp")
    z = kv // NY
    y = kv % NY
    R = 2 * NY * NZ
    D = NZ * NY * 2 * C

    def zpeer(k):
        return lax.rem(z + k, NZ)

    def ypeer(k):
        return lax.rem(y + k, NY)

    def at_z(zz):
        return {"kv": zz * NY + y}

    def at_y(yy):
        return {"kv": z * NY + yy}

    other = {"tp": 1 - t}

    def far_first(i):
        return NZ // 2 + (1 - 2 * lax.rem(i, 2)) * ((i + 1) // 2)

    barrier = pltpu.get_barrier_semaphore()

    def greet_z(i, c):
        pl.semaphore_signal(
            barrier, inc=1, device_id=at_z(zpeer(far_first(i))), device_id_type=pl.DeviceIdType.MESH
        )
        return c

    lax.fori_loop(0, NZ - 1, greet_z, 0)
    for k in range(1, NY):
        pl.semaphore_signal(
            barrier, inc=1, device_id=at_y(ypeer(k)), device_id_type=pl.DeviceIdType.MESH
        )
    pl.semaphore_signal(barrier, inc=1, device_id=other, device_id_type=pl.DeviceIdType.MESH)

    seq = lax.broadcasted_iota(jnp.int32, (R, R), 0)
    lane = lax.broadcasted_iota(jnp.int32, (R, R), 1)
    home = (lane % NZ) * (2 * NY) + (lane // (2 * NZ)) * 2 + (lane // NZ) % 2
    perm = jnp.where(seq == home, 1.0, 0.0).astype(BF16)
    s0[...] = dot(sT[...], perm, 1, 0).astype(BF16)

    def fold(wgu, wg, wu, gain):
        row = gain[...]
        pad = jnp.zeros((HID - FFL, D), F32)
        for part, w in enumerate((wg, wu)):
            scaled = jnp.concatenate([w[...].astype(F32) * row, pad], axis=0)
            wgu[part * HID : (part + 1) * HID, :] = scaled.astype(BF16)

    def turn(wdt, wd):
        width = NY * 2 * C
        for b in range(NZ):
            block = wd[:, b * width : (b + 1) * width].astype(F32)
            block = jnp.concatenate([block, jnp.zeros((128 - FFL, width), F32)], axis=0)
            turned = jnp.transpose(block).astype(BF16).reshape(NY, 2, C, 128)
            for p in range(2):
                for yy in range(NY):
                    wdt[p, yy, b] = turned[yy, p]

    fold(wgu1, wg1, wu1, g1)
    pl.semaphore_wait(barrier, NZ - 1 + NY - 1 + 1)

    sends = []

    def gather(phase, src, gat):
        def go(i, c):
            k = far_first(i)
            copy_to(
                src, gat.at[z, y, t], ag_z.at[phase, 0, k], ag_z.at[phase, 1, k], **at_z(zpeer(k))
            ).start()
            return c

        lax.fori_loop(0, NZ - 1, go, 0)
        gat[z, y, t] = src[...]

        def there(k, c):
            copy_to(
                src, gat.at[z, y, t], ag_z.at[phase, 0, k], ag_z.at[phase, 1, k], **at_z(zpeer(k))
            ).wait_recv()
            return c

        def drained(k, c):
            copy_to(
                src, gat.at[z, y, t], ag_z.at[phase, 0, k], ag_z.at[phase, 1, k], **at_z(zpeer(k))
            ).wait_send()
            return c

        sends.append(lambda: lax.fori_loop(1, NZ, drained, 0))
        return there

    def gather_rest(phase, gat, there):
        lax.fori_loop(1, NZ, there, 0)
        column = gat.at[:, y, t]
        ys = []
        for k in range(1, NY):
            c = copy_to(
                column, column, ag_y.at[phase, 0, k], ag_y.at[phase, 1, k], **at_y(ypeer(k))
            )
            c.start()
            ys.append(c)
        ts = []
        for k in range(NY):
            if k:
                ys[k - 1].wait_recv()
            theirs = gat.at[:, lax.rem(y + NY - k, NY), t]
            c = copy_to(theirs, theirs, ag_t.at[phase, 0, k], ag_t.at[phase, 1, k], **other)
            c.start()
            ts.append(c)
        for c in ts:
            c.wait_recv()
        sends.extend(c.wait_send for c in ys + ts)

    def half(phase, gat, wgu, wdt, s_own):
        rows = gat[...].reshape(D, R)
        acc = dot(wgu[...], rows, 1, 0)
        wide = rows.astype(F32)
        scale = lax.rsqrt(jnp.sum(wide * wide, axis=0, keepdims=True) / D + EPSILON)
        gate = acc[:HID] * scale
        up = acc[HID:] * scale
        hidden = (gate * jax.nn.sigmoid(gate) * up).astype(BF16)
        hidden = jnp.concatenate([hidden, jnp.zeros((128 - HID, R), BF16)], axis=0)
        ts = []
        for k in range(1, NY + 1):
            yy = lax.rem(y + k, NY)
            w = wdt[1 - t, yy].reshape(NZ * C, 128)
            psend[phase, k - 1] = dot(w, hidden, 1, 0).astype(BF16).reshape(NZ, C, R)
            c = copy_to(
                psend.at[phase, k - 1],
                ptp.at[phase, k - 1],
                rs_t.at[phase, 0, k - 1],
                rs_t.at[phase, 1, k - 1],
                **other,
            )
            c.start()
            ts.append(c)
        ys = []
        for k in range(1, NY + 1):
            yy = lax.rem(y + k, NY)
            w = wdt[t, yy].reshape(NZ * C, 128)
            mine = dot(w, hidden, 1, 0).reshape(NZ, C, R)
            ts[k - 1].wait_recv()
            both = mine + ptp[phase, k - 1].astype(F32)
            if k < NY:
                ysend[phase, k - 1] = both.astype(BF16)
                c = copy_to(
                    ysend.at[phase, k - 1],
                    yrecv.at[phase, k - 1],
                    rs_y.at[phase, 0, k - 1],
                    rs_y.at[phase, 1, k - 1],
                    **at_y(yy),
                )
                c.start()
                ys.append(c)
        for c in ys:
            c.wait_recv()
        for k in range(1, NY):
            both = both + yrecv[phase, k - 1].astype(F32)
        accf[phase] = both
        zsend[phase] = both.astype(BF16)

        def zcopy(k):
            zz = zpeer(k)
            return copy_to(
                zsend.at[phase, zz],
                zrecv.at[phase, k],
                rs_z.at[phase, 0, k],
                rs_z.at[phase, 1, k],
                **at_z(zz),
            )

        def go(i, c):
            zcopy(far_first(i)).start()
            return c

        def there(k, c):
            zcopy(k).wait_recv()
            return c

        def drained(k, c):
            zcopy(k).wait_send()
            return c

        lax.fori_loop(0, NZ - 1, go, 0)
        lax.fori_loop(1, NZ, there, 0)
        total = accf[phase, z]
        for k in range(1, NZ):
            total = total + zrecv[phase, k].astype(F32)
        sends.extend(c.wait_send for c in ts + ys)
        sends.append(lambda: lax.fori_loop(1, NZ, drained, 0))
        return (s_own + 0.5 * total).astype(BF16)

    there = gather(0, s0, gat1)
    turn(wdt1, wd1)
    fold(wgu2, wg2, wu2, g2)
    turn(wdt2, wd2)
    eye = lax.broadcasted_iota(jnp.int32, (2 * C, 2 * C), 0) == lax.broadcasted_iota(
        jnp.int32, (2 * C, 2 * C), 1
    )
    gain_col = jnp.sum(
        jnp.where(eye, jnp.broadcast_to(gm[...], (2 * C, 2 * C)), 0.0), axis=1, keepdims=True
    )
    gather_rest(0, gat1, there)
    middle = half(0, gat1, wgu1, wdt1, s0[...].astype(F32))

    pair[t] = middle
    c = copy_to(pair.at[t], pair.at[t], tp_s.at[0], tp_s.at[1], **other)
    c.start()
    c.wait_recv()
    sends.append(c.wait_send)

    wide = pair[...].astype(F32).reshape(2 * C, R)
    turned = jnp.transpose(wide)
    u2 = jnp.transpose(wide * gain_col).astype(BF16)
    f = 0
    for w in (wq, wk, wz, wv, wo):
        part = dot(u2, w[...], 1, 0).astype(BF16)
        for j in range(w.shape[1] // 128):
            psnd[:, f] = part[:, j * 128 : (j + 1) * 128].reshape(NY, 2 * NZ, 128)
            f += 1
    squares = jnp.sum(turned * turned, axis=1, keepdims=True)
    psnd[:, f] = jnp.broadcast_to(squares, (R, 128)).astype(BF16).reshape(NY, 2 * NZ, 128)
    ys = []
    for k in range(1, NY):
        yy = ypeer(k)
        c = copy_to(psnd.at[yy], prcv.at[k - 1], pr_y.at[0, k - 1], pr_y.at[1, k - 1], **at_y(yy))
        c.start()
        ys.append(c)
    for c in ys:
        c.wait_recv()
    sends.extend(c.wait_send for c in ys)
    for f in range(NF):
        chunk = psnd[y, f].astype(F32)
        for k in range(1, NY):
            chunk = chunk + prcv[k - 1, f].astype(F32)
        for s in range(2):
            zs[pl.ds(s * 16 + f, NZ, stride=32), :] = chunk[s * NZ : (s + 1) * NZ]
    for s in range(2):
        zs[pl.ds(s * 16 + NF, NZ, stride=32), :] = jnp.zeros((NZ, 128), F32)
    zsb[...] = zs[...].astype(BF16).reshape(NZ, 32, 128)

    def pcopy(k):
        zz = zpeer(k)
        return copy_to(zsb.at[zz], zrb.at[k], pr_z.at[0, k], pr_z.at[1, k], **at_z(zz))

    def pgo(i, c):
        pcopy(far_first(i)).start()
        return c

    def pthere(k, c):
        pcopy(k).wait_recv()
        return c

    def pdrained(k, c):
        pcopy(k).wait_send()
        return c

    lax.fori_loop(0, NZ - 1, pgo, 0)
    lax.fori_loop(1, NZ, pthere, 0)
    sends.append(lambda: lax.fori_loop(1, NZ, pdrained, 0))
    total = zs[pl.ds(pl.multiple_of(z * 32, 32), 32), :]
    for k in range(1, NZ):
        total = total + zrb[k].astype(F32)

    blocks = []
    columns = []
    for s in range(2):
        b = total[s * 16 : (s + 1) * 16]
        b = b * lax.rsqrt(b[NF - 1 : NF] / D + EPSILON)
        blocks.append(b)
        logits = b[4:6]
        amounts = jnp.concatenate([dec[s : s + 1, 0:128], dec[s : s + 1, 128:256]], axis=0)
        sig = jnp.minimum(logits, 0.0) - jnp.log(1.0 + jnp.exp(-jnp.abs(logits)))
        decay = jnp.exp(sig / GATE_SOFTNESS - amounts)
        columns += [b[0:2] * 0.125, b[2:4], decay]
    columns.append(jnp.zeros((128 - 12, 128), F32))
    cols = jnp.transpose(jnp.concatenate(columns, axis=0))
    rows = []
    for s in range(2):
        for h in range(4):
            lo = (h % 2) * 64
            q, k_, a = (
                cols[lo : lo + 64, s * 6 + 2 * i + h // 2 : s * 6 + 2 * i + h // 2 + 1]
                for i in range(3)
            )
            b = blocks[s]
            state = a * old[s, h] + k_ * b[6 + h : 7 + h]
            new[s, h] = state
            read = jnp.sum(q * state, axis=0, keepdims=True)
            normed = read * lax.rsqrt(jnp.mean(read * read, axis=1, keepdims=True) + EPSILON)
            o = b[10 + h : 11 + h]
            rows.append(normed * hg[h : h + 1] * (o * jax.nn.sigmoid(o)))
    mg[y, z] = jnp.concatenate(rows, axis=0).astype(BF16)

    def mcopy(k):
        own_block = mg.at[y, z]
        return copy_to(own_block, own_block, mh_z.at[0, k], mh_z.at[1, k], **at_z(zpeer(k)))

    def mgo(i, c):
        mcopy(far_first(i)).start()
        return c

    def mthere(k, c):
        mcopy(k).wait_recv()
        return c

    def mdrained(k, c):
        mcopy(k).wait_send()
        return c

    lax.fori_loop(0, NZ - 1, mgo, 0)
    lax.fori_loop(1, NZ, mthere, 0)
    sends.append(lambda: lax.fori_loop(1, NZ, mdrained, 0))
    ys = []
    for k in range(1, NY):
        c = copy_to(mg.at[y], mg.at[y], mh_y.at[0, k], mh_y.at[1, k], **at_y(ypeer(k)))
        c.start()
        ys.append(c)
    for c in ys:
        c.wait_recv()
    sends.extend(c.wait_send for c in ys)
    mgf[...] = mg[...].astype(F32).reshape(NY * NZ * 8, 128)
    heads = []
    for h in range(4):
        pieces = [
            mgf[pl.ds(yy * NZ * 8 + s * 4 + h, NZ, stride=8), :] for yy in range(NY) for s in range(2)
        ]
        heads.append(jnp.concatenate(pieces, axis=0))
    mixed = jnp.concatenate(heads, axis=1).astype(BF16)
    pj[...] = dot(wout[...], mixed, 1, 1).astype(BF16).reshape(2, C, R)
    c = copy_to(pj.at[1 - t], pjr, fin_s.at[0], fin_s.at[1], **other)
    c.start()
    c.wait_recv()
    sends.append(c.wait_send)
    attention = pj[t].astype(F32) + pjr[...].astype(F32)
    after = (middle.astype(F32) + attention).astype(BF16)
    aft[...] = after

    there = gather(1, aft, gat2)
    gather_rest(1, gat2, there)
    result = half(1, gat2, wgu2, wdt2, after.astype(F32))
    outT[...] = dot(result, perm, 1, 1).astype(BF16)
    for wait in sends:
        wait()


def body(
    stream,
    old_state,
    decay_amounts,
    first_gain,
    first_gate,
    first_up,
    first_down,
    mixer_gain,
    query_weight,
    key_weight,
    decay_weight,
    value_weight,
    output_gate_weight,
    head_gain,
    output_weight,
    second_gain,
    second_gate,
    second_up,
    second_down,
):
    NZ = lax.axis_size("kv") // NY
    R = 2 * NY * NZ
    D = NY * NZ * 2 * C
    V = pltpu.VMEM
    S = pltpu.SemaphoreType.DMA
    outT, new = pl.pallas_call(
        functools.partial(kernel, NZ, first_gate.shape[1]),
        out_shape=(
            jax.ShapeDtypeStruct((C, R), BF16),
            jax.ShapeDtypeStruct(old_state.shape, F32),
        ),
        in_specs=[pl.BlockSpec(memory_space=pltpu.VMEM)] * 19,
        out_specs=[pl.BlockSpec(memory_space=pltpu.VMEM)] * 2,
        scratch_shapes=[
            V((NZ, NY, 2, C, R), BF16),
            V((NZ, NY, 2, C, R), BF16),
            V((2 * HID, D), BF16),
            V((2 * HID, D), BF16),
            V((2, NY, NZ, C, 128), BF16),
            V((2, NY, NZ, C, 128), BF16),
            V((C, R), BF16),
            V((2, NY, NZ, C, R), BF16),
            V((8, 128), F32),
            V((2, NY, NZ, C, R), BF16),
            V((2, NY - 1, NZ, C, R), BF16),
            V((2, NY - 1, NZ, C, R), BF16),
            V((2, NZ, C, R), F32),
            V((2, NZ, C, R), BF16),
            V((2, NZ, C, R), BF16),
            V((2, C, R), BF16),
            V((NY, NF, 2 * NZ, 128), BF16),
            V((NY - 1, NF, 2 * NZ, 128), BF16),
            V((NZ * 32, 128), F32),
            V((NZ, 32, 128), BF16),
            V((NZ, 32, 128), BF16),
            V((NY, NZ, 8, 128), BF16),
            V((NY * NZ * 8, 128), F32),
            V((2, C, R), BF16),
            V((C, R), BF16),
            V((C, R), BF16),
            S((2, 2, NZ)),
            S((2, 2, NY)),
            S((2, 2, NY)),
            S((2, 2, NY)),
            S((2, 2, NY)),
            S((2, 2, NZ)),
            S((2,)),
            S((2, NY)),
            S((2, NZ)),
            S((2, NY)),
            S((2, NZ)),
            S((2,)),
        ],
        compiler_params=pltpu.CompilerParams(collective_id=0, has_side_effects=True),
        name="layer",
    )(
        stream.T,
        old_state,
        decay_amounts,
        first_gain.reshape(1, D),
        first_gate.T,
        first_up.T,
        first_down,
        mixer_gain.reshape(1, 2 * C),
        query_weight,
        key_weight,
        decay_weight,
        value_weight,
        output_gate_weight,
        head_gain.reshape(4, 128),
        output_weight.T,
        second_gain.reshape(1, D),
        second_gate.T,
        second_up.T,
        second_down,
    )
    return outT.T, new


def solution(mesh):
    in_specs = (
        P("dp", ("kv", "tp")),
        P(("dp", "kv"), "tp", None, None),
        P(("dp", "kv"), "tp"),
        P(),
        P(None, ("kv", "tp")),
        P(None, ("kv", "tp")),
        P(("kv", "tp"), None),
        P("kv"),
        P("kv", "tp"),
        P("kv", "tp"),
        P("kv", "tp"),
        P("kv", "tp"),
        P("kv", "tp"),
        P("tp"),
        P("tp", "kv"),
        P(),
        P(None, ("kv", "tp")),
        P(None, ("kv", "tp")),
        P(("kv", "tp"), None),
    )
    out_specs = (P("dp", ("kv", "tp")), P(("dp", "kv"), "tp", None, None))
    return jax.shard_map(body, mesh=mesh, in_specs=in_specs, out_specs=out_specs, check_vma=False)
```

time: 387 us -> 110 us (0.28)
  blocking collectives: 299 us -> 0 us
  Pallas kernels: 0 us -> 105 us
  waiting for transfers between devices: 52.7 us -> 0 us
  local copies, waits for them, and re-layouts: 14.2 us -> 2.94 us
  other arithmetic: 7.92 us -> 0 us
  starting transfers between devices: 5.97 us -> 0 us
    all_gather x2 -> x0, blocking collectives: 171 us -> none  [half_block(): lax.all_gather(stream, ('kv', 'tp'), axis=1, tiled=True).astype(jnp.float32)]
    all_to_all x9 -> x0, blocking collectives: 128 us -> none  [the longest x2 82.2 us: summed_on_arrival_2(): lax.all_to_all(parts, axis, split_axis=0, concat_axis=0, tiled=True)]
    pallas_call x0 -> x1, Pallas kernels: none -> 105 us  [body(): pl.pallas_call(functools.partial(kernel, NZ, first_gate.shape[1]), out_sh...]
    all_to_all x1 -> x0, waiting for transfers between devices: 52.7 us -> none  [summed_on_arrival_2(): lax.all_to_all(parts, axis, split_axis=0, concat_axis=0, tiled=True)]
    unnamed x48 -> x4, local copies, waits for them, and re-layouts: 9.67 us -> 2.94 us
    all_to_all x1 -> x0, starting transfers between devices: 5.97 us -> none  [summed_on_arrival_2(): lax.all_to_all(parts, axis, split_axis=0, concat_axis=0, tiled=True)]
    all_to_all x4 -> x0, other arithmetic: 5.12 us -> none  [the longest x2 3.77 us: summed_on_arrival_2(): lax.all_to_all(parts, axis, split_axis=0, concat_axis=0, tiled=True)]
  transfers between devices with their start and end apart: 1 -> 0, of which waited for: 1 -> 0; matrix products, arithmetic and copies ran while one was open for 0% -> 0% of each run, Pallas kernels for 0% -> 0%
where the time goes in v1:
time: 110 us; the launch traced here: 109 us
  Pallas kernels  105 us (95%)
  local copies, waits for them, and re-layouts  2.94 us (3%)
    pallas_call x1, Pallas kernels, body(): pl.pallas_call(functools.partial(kernel, NZ, first_gate.shape[1]), out_sh...  105 us
    unnamed x4, local copies, waits for them, and re-layouts  2.94 us

profile of v1, /device:TPU:6, one launch (start us, length us, event | category | flops | bytes accessed | tf_op | source)
XLA Modules:
  0.0 109.0 jit_solution(8202114288593061072)
XLA Ops:
  0.6 105.4 %layer.1 = (bf16[16,128]{1,0:T(8,128)(2,1)}, f32[2,4,64,128]{3,2,1,0:T(8,128)}) custom-call(bf16[16,128]{1,0:T(8,128)(2,1)} %bitcast.18, f32[2,4,64,128]{3,2,1,0:T(8,128)} %old.1, f32[2,256]{1,0:T(2,128)} %dec.1, f32[1,2048]{1,0:T(1,128)} %bitcast.16, bf16[44,2048]{1,0:T(8,128)(2,1)} %bitcast.11, bf16[44,2048]{1,0:T(8,128)(2,1)} %bitcast.12, ...), custom_call_target="tpu_custom_call" | custom-call | tf_op jit(solution)/shard_map/layer/pallas_call | solution.py:472
  106.0 0.0 copy-start
  106.0 0.7 copy-done
  106.7 0.6 copy.23
  107.3 1.7 %copy.24 = f32[2,4,64,128]{3,2,1,0:T(8,128)} copy(f32[2,4,64,128]{3,2,1,0:T(8,128)} %get-tuple-element.9) | data formatting | bytes 524288
Async XLA Ops:
  106.0 0.7 copy-start

commit v2 on v0

v2 whole, which is shorter than its diff:
```python
import functools

import jax
import jax.numpy as jnp
from jax import lax
from jax.experimental import pallas as pl
from jax.experimental.pallas import tpu as pltpu
from jax.sharding import PartitionSpec as P

EPSILON = 1e-06
GATE_SOFTNESS = 16.0
NY = 4
C = 16
HID = 48
NF = 15
F32 = jnp.float32
BF16 = jnp.bfloat16


def copy_to(src, dst, send, recv, **where):
    return pltpu.make_async_remote_copy(
        src_ref=src,
        dst_ref=dst,
        send_sem=send,
        recv_sem=recv,
        device_id=where,
        device_id_type=pl.DeviceIdType.MESH,
    )


def dot(a, b, ca, cb):
    return lax.dot_general(a, b, (((ca,), (cb,)), ((), ())), preferred_element_type=F32)


def kernel(NZ, FFL, *refs):
    hbm = refs[:19]
    outT, new = refs[19:21]
    local = refs[21:40]
    (
        newv,
        gat1,
        gat2,
        wgu1,
        wgu2,
        wdt1,
        wdt2,
        s0,
        psend,
        ptp,
        ysend,
        yrecv,
        accf,
        zsend,
        zrecv,
        midg,
        wall,
        wsh,
        zs,
        zsb,
        zrb,
        tot,
        ytot,
        mg,
        mgf,
        pj,
        pjr,
        ld,
        ag,
        ag_t,
        rs_t,
        rs_y,
        rs_z,
        md,
        w_y,
        pr_z,
        pr_y,
        mh,
        fin_s,
    ) = refs[40:]
    (
        sT,
        old,
        dec,
        g1,
        wg1,
        wu1,
        wd1,
        gm,
        wq,
        wk,
        wz,
        wv,
        wo,
        hg,
        wout,
        g2,
        wg2,
        wu2,
        wd2,
    ) = local
    kv = lax.axis_index("kv")
    t = lax.axis_index("tp")
    z = kv // NY
    y = kv % NY
    R = 2 * NY * NZ
    D = NZ * NY * 2 * C

    def zpeer(k):
        return lax.rem(z + k, NZ)

    def ypeer(k):
        return lax.rem(y + k, NY)

    def yfrom(k):
        return lax.rem(y + NY - k, NY)

    def at_z(zz):
        return {"kv": zz * NY + y}

    def at_y(yy):
        return {"kv": z * NY + yy}

    other = {"tp": 1 - t}

    def far_first(i):
        return NZ // 2 + (1 - 2 * lax.rem(i, 2)) * ((i + 1) // 2)

    barrier = pltpu.get_barrier_semaphore()

    def greet(**where):
        pl.semaphore_signal(
            barrier, inc=1, device_id=where, device_id_type=pl.DeviceIdType.MESH
        )

    def greet_z(i, c):
        greet(**at_z(zpeer(far_first(i))))
        return c

    lax.fori_loop(0, NZ - 1, greet_z, 0)
    for k in range(1, NY):
        greet(**at_y(ypeer(k)))
        greet(**at_y(ypeer(k)), **other)
    greet(**other)

    def load(i):
        return pltpu.make_async_copy(hbm[i], local[i], ld.at[i])

    for i in (0, 3, 4, 5, 6, 7, 8, 9, 10, 11, 12, 15, 16, 17, 18, 1, 2, 13, 14):
        load(i).start()

    seq = lax.broadcasted_iota(jnp.int32, (R, R), 0)
    lane = lax.broadcasted_iota(jnp.int32, (R, R), 1)
    home = (lane % NZ) * (2 * NY) + (lane // (2 * NZ)) * 2 + (lane // NZ) % 2
    perm = jnp.where(seq == home, 1.0, 0.0).astype(BF16)
    load(0).wait()
    s0[...] = dot(sT[...], perm, 1, 0).astype(BF16)

    def fold(wgu, wg, wu, gain):
        row = gain[...]
        pad = jnp.zeros((HID - FFL, D), F32)
        for part, w in enumerate((wg, wu)):
            scaled = jnp.concatenate([w[...].astype(F32) * row, pad], axis=0)
            wgu[part * HID : (part + 1) * HID, :] = scaled.astype(BF16)

    def turn(wdt, wd):
        width = NY * 2 * C
        for b in range(NZ):
            block = wd[:, b * width : (b + 1) * width].astype(F32)
            block = jnp.concatenate([block, jnp.zeros((128 - FFL, width), F32)], axis=0)
            turned = jnp.transpose(block).astype(BF16).reshape(NY, 2, C, 128)
            for p in range(2):
                for yy in range(NY):
                    wdt[p, yy, b] = turned[yy, p]

    for i in (3, 4, 5):
        load(i).wait()
    fold(wgu1, wg1, wu1, g1)
    load(6).wait()
    turn(wdt1, wd1)
    for i in range(7, 13):
        load(i).wait()
    eye = lax.broadcasted_iota(jnp.int32, (2 * C, 2 * C), 0) == lax.broadcasted_iota(
        jnp.int32, (2 * C, 2 * C), 1
    )
    gain_col = jnp.sum(
        jnp.where(eye, jnp.broadcast_to(gm[...], (2 * C, 2 * C)), 0.0), axis=1, keepdims=True
    )
    f = 0
    for w in (wq, wk, wz, wv, wo):
        scaled = (w[...].astype(F32) * gain_col).astype(BF16)
        for j in range(w.shape[1] // 128):
            wall[f] = scaled[:, j * 128 : (j + 1) * 128]
            f += 1
    for f in range(NF - 1, 4 * NY):
        wall[f] = jnp.zeros((2 * C, 128), BF16)
    pl.semaphore_wait(barrier, NZ - 1 + 2 * (NY - 1) + 1)

    sends = []

    def owe(ref, sem):
        sends.append(copy_to(ref, ref, sem, sem, **other).wait_send)

    def got(ref, sem):
        copy_to(ref, ref, sem, sem, **other).wait_recv()

    G = max(NZ // 4, 1)
    NG = NZ // G
    order = [0] + [(i + 1) // 2 if i % 2 else NG - i // 2 for i in range(1, NG)]

    def gather(slot, most, sem, everything=None, pair_sem=None):
        mine = slot(z, 1, y)

        def send(i, c):
            copy_to(mine, mine, sem.at[0], sem.at[1 + z // G], **at_z(zpeer(far_first(i)))).start()
            return c

        lax.fori_loop(0, NZ - 1, send, 0)
        owe(slot(0, NZ - 1, 0), sem.at[0])

        def finish():
            arrival = 2 + NG
            for i in range(NG):
                q = lax.rem(z // G + order[i], NG)
                n = G if i else G - 1
                if n:
                    got(slot(0, n, 0), sem.at[1 + q])
                group = slot(q * G, G, y)
                for j in (2, 1, 3):
                    copy_to(
                        group,
                        group,
                        sem.at[1 + NG],
                        sem.at[arrival + (j - 1) * NG + i],
                        **at_y(ypeer(j)),
                    ).start()
                if pair_sem is not None:
                    copy_to(group, group, pair_sem.at[0], pair_sem.at[1], **other).start()
            for i in range(NG):
                q = lax.rem(z // G + order[i], NG)
                for j in (1, 3, 2):
                    group = slot(q * G, G, yfrom(j))
                    got(group, sem.at[arrival + (j - 1) * NG + i])
                    if pair_sem is not None:
                        copy_to(group, group, pair_sem.at[0], pair_sem.at[1], **other).start()
            owe(most, sem.at[1 + NG])
            if pair_sem is not None:
                got(everything, pair_sem.at[1])
                owe(everything, pair_sem.at[0])

        return finish

    def half(phase, gat, wgu, wdt, s_own):
        rows = gat[...].reshape(D, R)
        acc = dot(wgu[...], rows, 1, 0)
        wide = rows.astype(F32)
        scale = lax.rsqrt(jnp.sum(wide * wide, axis=0, keepdims=True) / D + EPSILON)
        gate = acc[:HID] * scale
        up = acc[HID:] * scale
        hidden = (gate * jax.nn.sigmoid(gate) * up).astype(BF16)
        hidden = jnp.concatenate([hidden, jnp.zeros((128 - HID, R), BF16)], axis=0)
        ts = []
        for k in range(1, NY + 1):
            yy = lax.rem(y + k, NY)
            w = wdt[1 - t, yy].reshape(NZ * C, 128)
            psend[phase, k - 1] = dot(w, hidden, 1, 0).astype(BF16).reshape(NZ, C, R)
            c = copy_to(
                psend.at[phase, k - 1],
                ptp.at[phase, k - 1],
                rs_t.at[phase, 0],
                rs_t.at[phase, k],
                **other,
            )
            c.start()
            ts.append(c)
        for k in range(1, NY + 1):
            yy = lax.rem(y + k, NY)
            w = wdt[t, yy].reshape(NZ * C, 128)
            mine = dot(w, hidden, 1, 0).reshape(NZ, C, R)
            ts[k - 1].wait_recv()
            both = mine + ptp[phase, k - 1].astype(F32)
            if k < NY:
                ysend[phase, k - 1] = both.astype(BF16)
                c = copy_to(
                    ysend.at[phase, k - 1],
                    yrecv.at[phase, k - 1],
                    rs_y.at[phase, 0],
                    rs_y.at[phase, 1],
                    **at_y(yy),
                )
                c.start()
        owe(psend.at[phase], rs_t.at[phase, 0])
        owe(ysend.at[phase], rs_y.at[phase, 0])
        got(yrecv.at[phase], rs_y.at[phase, 1])
        for k in range(1, NY):
            both = both + yrecv[phase, k - 1].astype(F32)
        accf[phase] = both
        zsend[phase] = both.astype(BF16)
        total = scatter_z(
            zsend.at[phase], zrecv.at[phase], rs_z.at[phase], lambda: accf[phase, z]
        )
        return (s_own + 0.5 * total).astype(BF16)

    def scatter_z(source, landing, sem, mine):
        def send(i, c):
            k = far_first(i)
            zz = zpeer(k)
            copy_to(source.at[zz], landing.at[k], sem.at[0], sem.at[1], **at_z(zz)).start()
            return c

        lax.fori_loop(0, NZ - 1, send, 0)
        owe(landing.at[pl.ds(1, NZ - 1)], sem.at[0])
        total = mine()
        got(landing.at[pl.ds(1, NZ - 1)], sem.at[1])
        for k in range(1, NZ):
            total = total + landing[k].astype(F32)
        return total

    gat1[z, y, t] = s0[...]
    finish = gather(
        lambda zz, n, yy: gat1.at[pl.ds(zz, n), yy, t],
        gat1.at[:, pl.ds(0, NY - 1), t],
        ag.at[0],
        gat1.at[:, :, t],
        ag_t.at[0],
    )
    for k in range(1, NY):
        yy = ypeer(k)
        copy_to(wall.at[pl.ds(4 * yy, 4)], wsh.at[y], w_y.at[0], w_y.at[1], **at_y(yy)).start()
    owe(wall.at[pl.ds(0, 4 * (NY - 1))], w_y.at[0])
    wsh[y] = wall[pl.ds(4 * y, 4)]
    finish()
    for i in (15, 16, 17, 18):
        load(i).wait()
    middle = half(0, gat1, wgu1, wdt1, s0[...].astype(F32))

    here = midg.at[2 * y + t]
    here[...] = middle
    for k in range(NY):
        where = at_y(ypeer(k))
        copy_to(here, here, md.at[0], md.at[1], **where, **other).start()
        if k:
            copy_to(here, here, md.at[0], md.at[1], **where).start()
    most = midg.at[pl.ds(0, 2 * NY - 1)]
    owe(most, md.at[0])
    got(wsh.at[pl.ds(0, NY - 1)], w_y.at[1])
    got(most, md.at[1])

    turned = jnp.transpose(midg[...].astype(F32).reshape(NY * 2 * C, R))
    squares = jnp.sum(turned * turned, axis=1, keepdims=True)
    squares = squares * jnp.where(y == NY - 1, 1.0, 0.0)
    lhs = turned.astype(BF16)
    for c in range(4):
        part = dot(lhs, wsh[:, c].reshape(NY * 2 * C, 128), 1, 0)
        if c == 2:
            part = part + squares
        for yy in range(NY):
            for s in range(2):
                at = (yy * 2 + s) * NZ
                zs[pl.ds(yy * 8 + s * 4 + c, NZ, stride=32), :] = part[at : at + NZ]
    zsb[...] = zs[...].astype(BF16).reshape(NZ, 32, 128)
    total = scatter_z(
        zsb, zrb, pr_z, lambda: zs[pl.ds(pl.multiple_of(z * 32, 32), 32), :]
    )
    tot[...] = total.reshape(NY, 8, 128)
    for k in range(1, NY):
        yy = ypeer(k)
        copy_to(tot.at[yy], ytot.at[y], pr_y.at[0], pr_y.at[1], **at_y(yy)).start()
    owe(tot.at[pl.ds(0, NY - 1)], pr_y.at[0])
    ytot[y] = tot[y]
    for i in (1, 2, 13, 14):
        load(i).wait()
    got(tot.at[pl.ds(0, NY - 1)], pr_y.at[1])

    blocks = []
    columns = []
    for s in range(2):
        b = jnp.concatenate([ytot[yy, s * 4 : (s + 1) * 4] for yy in range(NY)], axis=0)
        b = b * lax.rsqrt(b[NF - 1 : NF] / D + EPSILON)
        blocks.append(b)
        logits = b[4:6]
        amounts = jnp.concatenate([dec[s : s + 1, 0:128], dec[s : s + 1, 128:256]], axis=0)
        sig = jnp.minimum(logits, 0.0) - jnp.log(1.0 + jnp.exp(-jnp.abs(logits)))
        decay = jnp.exp(sig / GATE_SOFTNESS - amounts)
        columns += [b[0:2] * 0.125, b[2:4], decay]
    columns.append(jnp.zeros((128 - 12, 128), F32))
    cols = jnp.transpose(jnp.concatenate(columns, axis=0))
    rows = []
    for s in range(2):
        for h in range(4):
            lo = (h % 2) * 64
            q, k_, a = (
                cols[lo : lo + 64, s * 6 + 2 * i + h // 2 : s * 6 + 2 * i + h // 2 + 1]
                for i in range(3)
            )
            b = blocks[s]
            state = a * old[s, h] + k_ * b[6 + h : 7 + h]
            newv[s, h] = state
            read = jnp.sum(q * state, axis=0, keepdims=True)
            normed = read * lax.rsqrt(jnp.mean(read * read, axis=1, keepdims=True) + EPSILON)
            o = b[10 + h : 11 + h]
            rows.append(normed * hg[h : h + 1] * (o * jax.nn.sigmoid(o)))
    mg[y, z] = jnp.concatenate(rows, axis=0).astype(BF16)

    finish = gather(lambda zz, n, yy: mg.at[yy, pl.ds(zz, n)], mg.at[pl.ds(0, NY - 1)], mh)
    out_copy = pltpu.make_async_copy(newv, new, ld.at[0])
    out_copy.start()
    sends.append(out_copy.wait)
    fold(wgu2, wg2, wu2, g2)
    turn(wdt2, wd2)
    finish()
    mgf[...] = mg[...].astype(F32).reshape(NY * NZ * 8, 128)
    heads = []
    for h in range(4):
        pieces = [
            mgf[pl.ds(yy * NZ * 8 + s * 4 + h, NZ, stride=8), :] for yy in range(NY) for s in range(2)
        ]
        heads.append(jnp.concatenate(pieces, axis=0))
    mixed = jnp.concatenate(heads, axis=1).astype(BF16)
    pj[...] = dot(wout[...], mixed, 1, 1).astype(BF16).reshape(2, C, R)
    c = copy_to(pj.at[1 - t], pjr, fin_s.at[0], fin_s.at[1], **other)
    c.start()
    sends.append(c.wait_send)
    c.wait_recv()
    attention = pj[t].astype(F32) + pjr[...].astype(F32)
    after = (middle.astype(F32) + attention).astype(BF16)

    gat2[z, y, t] = after
    gather(
        lambda zz, n, yy: gat2.at[pl.ds(zz, n), yy, t],
        gat2.at[:, pl.ds(0, NY - 1), t],
        ag.at[1],
        gat2.at[:, :, t],
        ag_t.at[1],
    )()
    result = half(1, gat2, wgu2, wdt2, after.astype(F32))
    outT[...] = dot(result, perm, 1, 1).astype(BF16)
    for wait in sends:
        wait()


def body(
    stream,
    old_state,
    decay_amounts,
    first_gain,
    first_gate,
    first_up,
    first_down,
    mixer_gain,
    query_weight,
    key_weight,
    decay_weight,
    value_weight,
    output_gate_weight,
    head_gain,
    output_weight,
    second_gain,
    second_gate,
    second_up,
    second_down,
):
    NZ = lax.axis_size("kv") // NY
    R = 2 * NY * NZ
    D = NY * NZ * 2 * C
    NG = NZ // max(NZ // 4, 1)
    V = pltpu.VMEM
    S = pltpu.SemaphoreType.DMA
    arrays = (
        stream.T,
        old_state,
        decay_amounts,
        first_gain.reshape(1, D),
        first_gate.T,
        first_up.T,
        first_down,
        mixer_gain.reshape(1, 2 * C),
        query_weight,
        key_weight,
        decay_weight,
        value_weight,
        output_gate_weight,
        head_gain.reshape(4, 128),
        output_weight.T,
        second_gain.reshape(1, D),
        second_gate.T,
        second_up.T,
        second_down,
    )
    outT, new = pl.pallas_call(
        functools.partial(kernel, NZ, first_gate.shape[1]),
        out_shape=(
            jax.ShapeDtypeStruct((C, R), BF16),
            jax.ShapeDtypeStruct(old_state.shape, F32),
        ),
        in_specs=[pl.BlockSpec(memory_space=pl.ANY)] * 19,
        out_specs=[pl.BlockSpec(memory_space=pltpu.VMEM), pl.BlockSpec(memory_space=pl.ANY)],
        scratch_shapes=[V(a.shape, a.dtype) for a in arrays]
        + [
            V(old_state.shape, F32),
            V((NZ, NY, 2, C, R), BF16),
            V((NZ, NY, 2, C, R), BF16),
            V((2 * HID, D), BF16),
            V((2 * HID, D), BF16),
            V((2, NY, NZ, C, 128), BF16),
            V((2, NY, NZ, C, 128), BF16),
            V((C, R), BF16),
            V((2, NY, NZ, C, R), BF16),
            V((2, NY, NZ, C, R), BF16),
            V((2, NY - 1, NZ, C, R), BF16),
            V((2, NY - 1, NZ, C, R), BF16),
            V((2, NZ, C, R), F32),
            V((2, NZ, C, R), BF16),
            V((2, NZ, C, R), BF16),
            V((2 * NY, C, R), BF16),
            V((4 * NY, 2 * C, 128), BF16),
            V((NY, 4, 2 * C, 128), BF16),
            V((NZ * 32, 128), F32),
            V((NZ, 32, 128), BF16),
            V((NZ, 32, 128), BF16),
            V((NY, 8, 128), F32),
            V((NY, 8, 128), F32),
            V((NY, NZ, 8, 128), BF16),
            V((NY * NZ * 8, 128), F32),
            V((2, C, R), BF16),
            V((C, R), BF16),
            S((19,)),
            S((2, 2 + NY * NG)),
            S((2, 2)),
            S((2, 1 + NY)),
            S((2, 2)),
            S((2, 2)),
            S((2,)),
            S((2,)),
            S((2,)),
            S((2,)),
            S((2 + NY * NG,)),
            S((2,)),
        ],
        compiler_params=pltpu.CompilerParams(collective_id=0, has_side_effects=True),
        name="layer",
    )(*arrays)
    return outT.T, new


def solution(mesh):
    in_specs = (
        P("dp", ("kv", "tp")),
        P(("dp", "kv"), "tp", None, None),
        P(("dp", "kv"), "tp"),
        P(),
        P(None, ("kv", "tp")),
        P(None, ("kv", "tp")),
        P(("kv", "tp"), None),
        P("kv"),
        P("kv", "tp"),
        P("kv", "tp"),
        P("kv", "tp"),
        P("kv", "tp"),
        P("kv", "tp"),
        P("tp"),
        P("tp", "kv"),
        P(),
        P(None, ("kv", "tp")),
        P(None, ("kv", "tp")),
        P(("kv", "tp"), None),
    )
    out_specs = (P("dp", ("kv", "tp")), P(("dp", "kv"), "tp", None, None))
    return jax.shard_map(body, mesh=mesh, in_specs=in_specs, out_specs=out_specs, check_vma=False)
```

time: 387 us -> 101 us (0.26)
  blocking collectives: 299 us -> 0 us
  Pallas kernels: 0 us -> 96.9 us
  waiting for transfers between devices: 52.7 us -> 0 us
  local copies, waits for them, and re-layouts: 14.2 us -> 2.94 us
  other arithmetic: 7.92 us -> 0 us
  starting transfers between devices: 5.97 us -> 0 us
    all_gather x2 -> x0, blocking collectives: 171 us -> none  [half_block(): lax.all_gather(stream, ('kv', 'tp'), axis=1, tiled=True).astype(jnp.float32)]
    all_to_all x9 -> x0, blocking collectives: 128 us -> none  [the longest x2 82.2 us: summed_on_arrival_2(): lax.all_to_all(parts, axis, split_axis=0, concat_axis=0, tiled=True)]
    pallas_call x0 -> x1, Pallas kernels: none -> 96.9 us  [body(): pl.pallas_call(functools.partial(kernel, NZ, first_gate.shape[1]), out_sh...]
    all_to_all x1 -> x0, waiting for transfers between devices: 52.7 us -> none  [summed_on_arrival_2(): lax.all_to_all(parts, axis, split_axis=0, concat_axis=0, tiled=True)]
    unnamed x48 -> x4, local copies, waits for them, and re-layouts: 9.67 us -> 2.94 us
    all_to_all x1 -> x0, starting transfers between devices: 5.97 us -> none  [summed_on_arrival_2(): lax.all_to_all(parts, axis, split_axis=0, concat_axis=0, tiled=True)]
    all_to_all x4 -> x0, other arithmetic: 5.12 us -> none  [the longest x2 3.77 us: summed_on_arrival_2(): lax.all_to_all(parts, axis, split_axis=0, concat_axis=0, tiled=True)]
  transfers between devices with their start and end apart: 1 -> 0, of which waited for: 1 -> 0; matrix products, arithmetic and copies ran while one was open for 0% -> 0% of each run, Pallas kernels for 0% -> 0%
where the time goes in v2:
time: 101 us
  Pallas kernels  96.9 us (96%)
  local copies, waits for them, and re-layouts  2.94 us (3%)
    pallas_call x1, Pallas kernels, body(): pl.pallas_call(functools.partial(kernel, NZ, first_gate.shape[1]), out_sh...  96.9 us
    unnamed x4, local copies, waits for them, and re-layouts  2.94 us

profile of v2, /device:TPU:6, one launch (start us, length us, event | category | flops | bytes accessed | tf_op | source)
XLA Modules:
  0.0 100.5 jit_solution(6133996500731560234)
XLA Ops:
  0.6 96.9 %layer.1 = (bf16[16,128]{1,0:T(8,128)(2,1)}, f32[2,4,64,128]{3,2,1,0:T(8,128)}) custom-call(bf16[16,128]{1,0:T(8,128)(2,1)} %bitcast.18, f32[2,4,64,128]{3,2,1,0:T(8,128)} %refs_1_.1, f32[2,256]{1,0:T(2,128)} %refs_2_.1, f32[1,2048]{1,0:T(1,128)} %bitcast.16, bf16[44,2048]{1,0:T(8,128)(2,1)} %bitcast.11, bf16[44,2048]{1,0:T(8,128)(2,1)} %bitcast.12, ...), custom_call_target="tpu_custom_call" | custom-call | tf_op jit(solution)/shard_map/layer/pallas_call | solution.py:489
  97.6 0.0 copy-start
  97.6 0.7 copy-done
  98.3 0.6 copy.23
  98.9 1.7 %copy.24 = f32[2,4,64,128]{3,2,1,0:T(8,128)} copy(f32[2,4,64,128]{3,2,1,0:T(8,128)} %get-tuple-element.9) | data formatting | bytes 524288
Async XLA Ops:
  97.6 0.7 copy-start

commit v3 on v2

--- a/solution.py
+++ b/solution.py
@@ -55,6 +55,8 @@
         midg,
         wall,
         wsh,
+        wog,
+        trn,
         zs,
         zsb,
         zrb,
@@ -64,6 +66,7 @@
         mgf,
         pj,
         pjr,
+        aft,
         ld,
         ag,
         ag_t,
@@ -72,6 +75,7 @@
         rs_z,
         md,
         w_y,
+        wo_y,
         pr_z,
         pr_y,
         mh,
@@ -161,6 +165,8 @@
         for part, w in enumerate((wg, wu)):
             scaled = jnp.concatenate([w[...].astype(F32) * row, pad], axis=0)
             wgu[part * HID : (part + 1) * HID, :] = scaled.astype(BF16)
+        if wgu.shape[0] > 2 * HID:
+            wgu[2 * HID :, :] = jnp.zeros((wgu.shape[0] - 2 * HID, D), BF16)
 
     def turn(wdt, wd):
         width = NY * 2 * C
@@ -249,56 +255,71 @@
 
         return finish
 
-    def half(phase, gat, wgu, wdt, s_own):
-        rows = gat[...].reshape(D, R)
-        acc = dot(wgu[...], rows, 1, 0)
-        wide = rows.astype(F32)
-        scale = lax.rsqrt(jnp.sum(wide * wide, axis=0, keepdims=True) / D + EPSILON)
-        gate = acc[:HID] * scale
-        up = acc[HID:] * scale
+    def gated(gate, up):
         hidden = (gate * jax.nn.sigmoid(gate) * up).astype(BF16)
-        hidden = jnp.concatenate([hidden, jnp.zeros((128 - HID, R), BF16)], axis=0)
-        ts = []
+        return jnp.concatenate([hidden, jnp.zeros((128 - HID, R), BF16)], axis=0)
+
+    def half(phase, hidden, wdt, meanwhile, residual):
         for k in range(1, NY + 1):
             yy = lax.rem(y + k, NY)
             w = wdt[1 - t, yy].reshape(NZ * C, 128)
             psend[phase, k - 1] = dot(w, hidden, 1, 0).astype(BF16).reshape(NZ, C, R)
-            c = copy_to(
+            copy_to(
                 psend.at[phase, k - 1],
                 ptp.at[phase, k - 1],
                 rs_t.at[phase, 0],
                 rs_t.at[phase, k],
                 **other,
-            )
-            c.start()
-            ts.append(c)
+            ).start()
+        owe(psend.at[phase], rs_t.at[phase, 0])
+        far = [(i, pl.ds(lax.rem(z // G + o, NG) * G, G)) for i, o in enumerate(order[::-1])]
         for k in range(1, NY + 1):
             yy = lax.rem(y + k, NY)
             w = wdt[t, yy].reshape(NZ * C, 128)
             mine = dot(w, hidden, 1, 0).reshape(NZ, C, R)
-            ts[k - 1].wait_recv()
+            got(ptp.at[phase, k - 1], rs_t.at[phase, k])
             both = mine + ptp[phase, k - 1].astype(F32)
             if k < NY:
                 ysend[phase, k - 1] = both.astype(BF16)
-                c = copy_to(
-                    ysend.at[phase, k - 1],
-                    yrecv.at[phase, k - 1],
-                    rs_y.at[phase, 0],
-                    rs_y.at[phase, 1],
-                    **at_y(yy),
-                )
-                c.start()
-        owe(psend.at[phase], rs_t.at[phase, 0])
+                for i, part in far:
+                    copy_to(
+                        ysend.at[phase, k - 1, part],
+                        yrecv.at[phase, k - 1, part],
+                        rs_y.at[phase, 0],
+                        rs_y.at[phase, 1 + i],
+                        **at_y(yy),
+                    ).start()
+        accf[phase] = both
         owe(ysend.at[phase], rs_y.at[phase, 0])
-        got(yrecv.at[phase], rs_y.at[phase, 1])
-        for k in range(1, NY):
-            both = both + yrecv[phase, k - 1].astype(F32)
-        accf[phase] = both
-        zsend[phase] = both.astype(BF16)
-        total = scatter_z(
-            zsend.at[phase], zrecv.at[phase], rs_z.at[phase], lambda: accf[phase, z]
-        )
-        return (s_own + 0.5 * total).astype(BF16)
+        for i, part in far:
+            got(yrecv.at[phase, :, part], rs_y.at[phase, 1 + i])
+            sums = accf[phase, part]
+            for k in range(1, NY):
+                sums = sums + yrecv[phase, k - 1, part].astype(F32)
+            accf[phase, part] = sums
+            zsend[phase, part] = sums.astype(BF16)
+            for j in range(G):
+                if i < NG - 1:
+                    zz = part.start + j
+                elif j:
+                    zz = part.start + lax.rem(z + j, G)
+                else:
+                    continue
+                copy_to(
+                    zsend.at[phase, zz],
+                    zrecv.at[phase, lax.rem(zz + NZ - z, NZ)],
+                    rs_z.at[phase, 0],
+                    rs_z.at[phase, 1],
+                    **at_z(zz),
+                ).start()
+        landed = zrecv.at[phase, pl.ds(1, NZ - 1)]
+        owe(landed, rs_z.at[phase, 0])
+        meanwhile()
+        total = accf[phase, z]
+        got(landed, rs_z.at[phase, 1])
+        for k in range(1, NZ):
+            total = total + zrecv[phase, k].astype(F32)
+        return (residual() + 0.5 * total).astype(BF16)
 
     def scatter_z(source, landing, sem, mine):
         def send(i, c):
@@ -323,15 +344,26 @@
         gat1.at[:, :, t],
         ag_t.at[0],
     )
-    for k in range(1, NY):
-        yy = ypeer(k)
-        copy_to(wall.at[pl.ds(4 * yy, 4)], wsh.at[y], w_y.at[0], w_y.at[1], **at_y(yy)).start()
-    owe(wall.at[pl.ds(0, 4 * (NY - 1))], w_y.at[0])
     wsh[y] = wall[pl.ds(4 * y, 4)]
     finish()
-    for i in (15, 16, 17, 18):
-        load(i).wait()
-    middle = half(0, gat1, wgu1, wdt1, s0[...].astype(F32))
+    all_rows = gat1[...].reshape(D, R)
+    acc = dot(wgu1[...], all_rows, 1, 0)
+    wide = all_rows.astype(F32)
+    scale = lax.rsqrt(jnp.sum(wide * wide, axis=0, keepdims=True) / D + EPSILON)
+
+    def share_weights():
+        for k in range(1, NY):
+            yy = ypeer(k)
+            copy_to(wall.at[pl.ds(4 * yy, 4)], wsh.at[y], w_y.at[0], w_y.at[1], **at_y(yy)).start()
+        load(14).wait()
+        for k in range(1, NY):
+            copy_to(wout, wog.at[y], wo_y.at[0], wo_y.at[1], **at_y(ypeer(k))).start()
+        owe(wall.at[pl.ds(0, 4 * (NY - 1))], w_y.at[0])
+        owe(wog.at[pl.ds(0, NY - 1)], wo_y.at[0])
+        wog[y] = wout[...]
+
+    hidden = gated(acc[:HID] * scale, acc[HID:] * scale)
+    middle = half(0, hidden, wdt1, share_weights, lambda: s0[...].astype(F32))
 
     here = midg.at[2 * y + t]
     here[...] = middle
@@ -346,6 +378,7 @@
     got(most, md.at[1])
 
     turned = jnp.transpose(midg[...].astype(F32).reshape(NY * 2 * C, R))
+    trn[...] = turned.reshape(2 * NY, NZ, 128)
     squares = jnp.sum(turned * turned, axis=1, keepdims=True)
     squares = squares * jnp.where(y == NY - 1, 1.0, 0.0)
     lhs = turned.astype(BF16)
@@ -367,7 +400,7 @@
         copy_to(tot.at[yy], ytot.at[y], pr_y.at[0], pr_y.at[1], **at_y(yy)).start()
     owe(tot.at[pl.ds(0, NY - 1)], pr_y.at[0])
     ytot[y] = tot[y]
-    for i in (1, 2, 13, 14):
+    for i in (1, 2, 13):
         load(i).wait()
     got(tot.at[pl.ds(0, NY - 1)], pr_y.at[1])
 
@@ -399,32 +432,38 @@
             normed = read * lax.rsqrt(jnp.mean(read * read, axis=1, keepdims=True) + EPSILON)
             o = b[10 + h : 11 + h]
             rows.append(normed * hg[h : h + 1] * (o * jax.nn.sigmoid(o)))
-    mg[y, z] = jnp.concatenate(rows, axis=0).astype(BF16)
-
-    finish = gather(lambda zz, n, yy: mg.at[yy, pl.ds(zz, n)], mg.at[pl.ds(0, NY - 1)], mh)
+    mg[z] = jnp.concatenate(rows, axis=0).astype(BF16)
+
+    def send_heads(i, c):
+        zz = zpeer(far_first(i))
+        copy_to(mg.at[z], mg.at[z], mh.at[0], mh.at[1], **at_z(zz)).start()
+        return c
+
+    lax.fori_loop(0, NZ - 1, send_heads, 0)
+    owe(mg.at[pl.ds(0, NZ - 1)], mh.at[0])
     out_copy = pltpu.make_async_copy(newv, new, ld.at[0])
     out_copy.start()
     sends.append(out_copy.wait)
+    for i in (15, 16, 17, 18):
+        load(i).wait()
     fold(wgu2, wg2, wu2, g2)
     turn(wdt2, wd2)
-    finish()
-    mgf[...] = mg[...].astype(F32).reshape(NY * NZ * 8, 128)
+    got(wog.at[pl.ds(0, NY - 1)], wo_y.at[1])
+    got(mg.at[pl.ds(0, NZ - 1)], mh.at[1])
+    mgf[...] = mg[...].astype(F32).reshape(NZ * 8, 128)
     heads = []
     for h in range(4):
-        pieces = [
-            mgf[pl.ds(yy * NZ * 8 + s * 4 + h, NZ, stride=8), :] for yy in range(NY) for s in range(2)
-        ]
+        pieces = [mgf[pl.ds(s * 4 + h, NZ, stride=8), :] for s in range(2)]
         heads.append(jnp.concatenate(pieces, axis=0))
     mixed = jnp.concatenate(heads, axis=1).astype(BF16)
-    pj[...] = dot(wout[...], mixed, 1, 1).astype(BF16).reshape(2, C, R)
-    c = copy_to(pj.at[1 - t], pjr, fin_s.at[0], fin_s.at[1], **other)
-    c.start()
-    sends.append(c.wait_send)
-    c.wait_recv()
+    product = dot(mixed, wog[...].reshape(NY * 2 * C, 512), 1, 1).astype(BF16)
+    pj[...] = product.reshape(2, NZ, NY * 2 * C)
+    copy_to(pj.at[1 - t], pjr, fin_s.at[0], fin_s.at[1], **other).start()
+    owe(pjr, fin_s.at[0])
+    got(pjr, fin_s.at[1])
     attention = pj[t].astype(F32) + pjr[...].astype(F32)
-    after = (middle.astype(F32) + attention).astype(BF16)
-
-    gat2[z, y, t] = after
+
+    gat2[z, y, t] = (trn[2 * y + t] + attention).astype(BF16)
     gather(
         lambda zz, n, yy: gat2.at[pl.ds(zz, n), yy, t],
         gat2.at[:, pl.ds(0, NY - 1), t],
@@ -432,7 +471,18 @@
         gat2.at[:, :, t],
         ag_t.at[1],
     )()
-    result = half(1, gat2, wgu2, wdt2, after.astype(F32))
+    all_rows = jnp.concatenate([gat2[i].reshape(R, NY * 2 * C) for i in range(NZ)], axis=1)
+    acc = dot(all_rows, wgu2[...], 1, 1)
+    wide = all_rows.astype(F32)
+    scale = lax.rsqrt(jnp.sum(wide * wide, axis=1, keepdims=True) / D + EPSILON)
+    acc = jnp.transpose(acc * scale)
+
+    def own_columns():
+        block = gat2[z].astype(F32).reshape(R, NY * 2 * C)
+        aft[...] = jnp.transpose(block).reshape(2 * NY, C, R)
+
+    hidden = gated(acc[:HID], acc[HID : 2 * HID])
+    result = half(1, hidden, wdt2, own_columns, lambda: aft[2 * y + t])
     outT[...] = dot(result, perm, 1, 1).astype(BF16)
     for wait in sends:
         wait()
@@ -498,9 +548,9 @@
         + [
             V(old_state.shape, F32),
             V((NZ, NY, 2, C, R), BF16),
-            V((NZ, NY, 2, C, R), BF16),
+            V((NZ, NY, 2, NZ, NY * 2 * C), BF16),
             V((2 * HID, D), BF16),
-            V((2 * HID, D), BF16),
+            V((128, D), BF16),
             V((2, NY, NZ, C, 128), BF16),
             V((2, NY, NZ, C, 128), BF16),
             V((C, R), BF16),
@@ -514,26 +564,30 @@
             V((2 * NY, C, R), BF16),
             V((4 * NY, 2 * C, 128), BF16),
             V((NY, 4, 2 * C, 128), BF16),
+            V((NY, 2 * C, 512), BF16),
+            V((2 * NY, NZ, 128), F32),
             V((NZ * 32, 128), F32),
             V((NZ, 32, 128), BF16),
             V((NZ, 32, 128), BF16),
             V((NY, 8, 128), F32),
             V((NY, 8, 128), F32),
-            V((NY, NZ, 8, 128), BF16),
-            V((NY * NZ * 8, 128), F32),
-            V((2, C, R), BF16),
-            V((C, R), BF16),
+            V((NZ, 8, 128), BF16),
+            V((NZ * 8, 128), F32),
+            V((2, NZ, NY * 2 * C), BF16),
+            V((NZ, NY * 2 * C), BF16),
+            V((2 * NY, C, R), F32),
             S((19,)),
             S((2, 2 + NY * NG)),
             S((2, 2)),
             S((2, 1 + NY)),
-            S((2, 2)),
+            S((2, 1 + NG)),
             S((2, 2)),
             S((2,)),
             S((2,)),
             S((2,)),
             S((2,)),
-            S((2 + NY * NG,)),
+            S((2,)),
+            S((2,)),
             S((2,)),
         ],
         compiler_params=pltpu.CompilerParams(collective_id=0, has_side_effects=True),

time: 101 us -> 95.7 us (0.948)
  Pallas kernels: 96.9 us -> 91.6 us
    pallas_call x1, Pallas kernels: 96.9 us -> 91.6 us  [body(): pl.pallas_call(functools.partial(kernel, NZ, first_gate.shape[1]), out_sh...]
where the time goes in v3:
time: 95.7 us; the launch traced here: 95.2 us
  Pallas kernels  91.6 us (96%)
  local copies, waits for them, and re-layouts  2.94 us (3%)
    pallas_call x1, Pallas kernels, body(): pl.pallas_call(functools.partial(kernel, NZ, first_gate.shape[1]), out_sh...  91.6 us
    unnamed x4, local copies, waits for them, and re-layouts  2.94 us

profile of v3, /device:TPU:6, one launch (start us, length us, event | category | flops | bytes accessed | tf_op | source)
XLA Modules:
  0.0 95.2 jit_solution(14275207382895141782)
XLA Ops:
  0.6 91.6 %layer.1 = (bf16[16,128]{1,0:T(8,128)(2,1)}, f32[2,4,64,128]{3,2,1,0:T(8,128)}) custom-call(bf16[16,128]{1,0:T(8,128)(2,1)} %bitcast.18, f32[2,4,64,128]{3,2,1,0:T(8,128)} %refs_1_.1, f32[2,256]{1,0:T(2,128)} %refs_2_.1, f32[1,2048]{1,0:T(1,128)} %bitcast.16, bf16[44,2048]{1,0:T(8,128)(2,1)} %bitcast.11, bf16[44,2048]{1,0:T(8,128)(2,1)} %bitcast.12, ...), custom_call_target="tpu_custom_call" | custom-call | tf_op jit(solution)/shard_map/layer/pallas_call | solution.py:539
  92.3 0.0 copy-start
  92.3 0.7 copy-done
  92.9 0.6 copy.23
  93.5 1.7 %copy.24 = f32[2,4,64,128]{3,2,1,0:T(8,128)} copy(f32[2,4,64,128]{3,2,1,0:T(8,128)} %get-tuple-element.9) | data formatting | bytes 524288
Async XLA Ops:
  92.3 0.7 copy-start

commit v4 on v3

--- a/solution.py
+++ b/solution.py
@@ -60,7 +60,6 @@
         zs,
         zsb,
         zrb,
-        tot,
         ytot,
         mg,
         mgf,
@@ -77,7 +76,6 @@
         w_y,
         wo_y,
         pr_z,
-        pr_y,
         mh,
         fin_s,
     ) = refs[40:]
@@ -321,21 +319,6 @@
             total = total + zrecv[phase, k].astype(F32)
         return (residual() + 0.5 * total).astype(BF16)
 
-    def scatter_z(source, landing, sem, mine):
-        def send(i, c):
-            k = far_first(i)
-            zz = zpeer(k)
-            copy_to(source.at[zz], landing.at[k], sem.at[0], sem.at[1], **at_z(zz)).start()
-            return c
-
-        lax.fori_loop(0, NZ - 1, send, 0)
-        owe(landing.at[pl.ds(1, NZ - 1)], sem.at[0])
-        total = mine()
-        got(landing.at[pl.ds(1, NZ - 1)], sem.at[1])
-        for k in range(1, NZ):
-            total = total + landing[k].astype(F32)
-        return total
-
     gat1[z, y, t] = s0[...]
     finish = gather(
         lambda zz, n, yy: gat1.at[pl.ds(zz, n), yy, t],
@@ -390,19 +373,32 @@
             for s in range(2):
                 at = (yy * 2 + s) * NZ
                 zs[pl.ds(yy * 8 + s * 4 + c, NZ, stride=32), :] = part[at : at + NZ]
-    zsb[...] = zs[...].astype(BF16).reshape(NZ, 32, 128)
-    total = scatter_z(
-        zsb, zrb, pr_z, lambda: zs[pl.ds(pl.multiple_of(z * 32, 32), 32), :]
-    )
-    tot[...] = total.reshape(NY, 8, 128)
-    for k in range(1, NY):
-        yy = ypeer(k)
-        copy_to(tot.at[yy], ytot.at[y], pr_y.at[0], pr_y.at[1], **at_y(yy)).start()
-    owe(tot.at[pl.ds(0, NY - 1)], pr_y.at[0])
-    ytot[y] = tot[y]
+    zsb[...] = zs[...].astype(BF16).reshape(NZ, NY, 8, 128)
+
+    def send_sums(i, c):
+        k = far_first(i)
+        zz = zpeer(k)
+        for j in (2, 1, 3, 0):
+            yy = ypeer(j)
+            there = {"kv": zz * NY + yy}
+            copy_to(zsb.at[zz, yy], zrb.at[k * NY + y], pr_z.at[0], pr_z.at[1], **there).start()
+        return c
+
+    lax.fori_loop(0, NZ - 1, send_sums, 0)
+    for j in (2, 1, 3):
+        yy = ypeer(j)
+        copy_to(zsb.at[z, yy], zrb.at[y], pr_z.at[0], pr_z.at[1], **at_y(yy)).start()
+    zrb[y] = zsb[z, y]
+    landed = zrb.at[pl.ds(0, NZ * NY - 1)]
+    owe(landed, pr_z.at[0])
     for i in (1, 2, 13):
         load(i).wait()
-    got(tot.at[pl.ds(0, NY - 1)], pr_y.at[1])
+    got(landed, pr_z.at[1])
+    for yy in range(NY):
+        total = zrb[yy].astype(F32)
+        for k in range(1, NZ):
+            total = total + zrb[k * NY + yy].astype(F32)
+        ytot[yy] = total
 
     blocks = []
     columns = []
@@ -486,6 +482,20 @@
     outT[...] = dot(result, perm, 1, 1).astype(BF16)
     for wait in sends:
         wait()
+
+
+def write_out(outT, new, outT_ref, new_ref, o_v, n_v, sem):
+    parts = new.shape[0]
+    moves = [(outT, o_v, outT_ref)] + [(new.at[i], n_v.at[i], new_ref.at[i]) for i in range(parts)]
+    ins = [pltpu.make_async_copy(a, v, sem.at[0, i]) for i, (a, v, _) in enumerate(moves)]
+    outs = [pltpu.make_async_copy(v, b, sem.at[1, i]) for i, (_, v, b) in enumerate(moves)]
+    for c in ins:
+        c.start()
+    for a, b in zip(ins, outs):
+        a.wait()
+        b.start()
+    for c in outs:
+        c.wait()
 
 
 def body(
@@ -567,9 +577,8 @@
             V((NY, 2 * C, 512), BF16),
             V((2 * NY, NZ, 128), F32),
             V((NZ * 32, 128), F32),
-            V((NZ, 32, 128), BF16),
-            V((NZ, 32, 128), BF16),
-            V((NY, 8, 128), F32),
+            V((NZ, NY, 8, 128), BF16),
+            V((NZ * NY, 8, 128), BF16),
             V((NY, 8, 128), F32),
             V((NZ, 8, 128), BF16),
             V((NZ * 8, 128), F32),
@@ -588,11 +597,21 @@
             S((2,)),
             S((2,)),
             S((2,)),
-            S((2,)),
         ],
         compiler_params=pltpu.CompilerParams(collective_id=0, has_side_effects=True),
         name="layer",
     )(*arrays)
+    outT, new = pl.pallas_call(
+        write_out,
+        out_shape=(
+            jax.ShapeDtypeStruct(outT.shape, BF16),
+            jax.ShapeDtypeStruct(new.shape, F32),
+        ),
+        in_specs=[pl.BlockSpec(memory_space=pl.ANY)] * 2,
+        out_specs=[pl.BlockSpec(memory_space=pl.ANY)] * 2,
+        scratch_shapes=[V(outT.shape, BF16), V(new.shape, F32), S((2, 1 + new.shape[0]))],
+        name="write_out",
+    )(outT, new)
     return outT.T, new
 
 

time: 95.7 us -> 92 us (0.961)
  local copies, waits for them, and re-layouts: 2.94 us -> 0 us
    unnamed x4 -> x0, local copies, waits for them, and re-layouts: 2.94 us -> none
    pallas_call x1, Pallas kernels: 91.6 us -> 89.5 us  [body(): pl.pallas_call(functools.partial(kernel, NZ, first_gate.shape[1]), out_sh...]
    pallas_call x0 -> x1, Pallas kernels: none -> 1.68 us  [body(): pl.pallas_call(write_out, out_shape=(jax.ShapeDtypeStruct(outT.shape, BF1...]
where the time goes in v4:
time: 92 us; the launch traced here: 91.8 us
  Pallas kernels  91.2 us (99%)
    pallas_call x1, Pallas kernels, body(): pl.pallas_call(functools.partial(kernel, NZ, first_gate.shape[1]), out_sh...  89.5 us

profile of v4, /device:TPU:6, one launch (start us, length us, event | category | flops | bytes accessed | tf_op | source)
XLA Modules:
  0.0 91.8 jit_solution(2064664472207816450)
XLA Ops:
  0.6 89.5 %layer.1 = (bf16[16,128]{1,0:T(8,128)(2,1)}, f32[2,4,64,128]{3,2,1,0:T(8,128)}) custom-call(bf16[16,128]{1,0:T(8,128)(2,1)} %bitcast.18, f32[2,4,64,128]{3,2,1,0:T(8,128)} %refs_1_.1, f32[2,256]{1,0:T(2,128)} %refs_2_.1, f32[1,2048]{1,0:T(1,128)} %bitcast.16, bf16[44,2048]{1,0:T(8,128)(2,1)} %bitcast.11, bf16[44,2048]{1,0:T(8,128)(2,1)} %bitcast.12, ...), custom_call_target="tpu_custom_call" | custom-call | tf_op jit(solution)/shard_map/layer/pallas_call | solution.py:549
  90.1 1.7 %write_out.1 = (bf16[16,128]{1,0:T(8,128)(2,1)}, f32[2,4,64,128]{3,2,1,0:T(8,128)}) custom-call(bf16[16,128]{1,0:T(8,128)(2,1)} %get-tuple-element.6.outT, f32[2,4,64,128]{3,2,1,0:T(8,128)} %get-tuple-element.7.new), custom_call_target="tpu_custom_call" | custom-call | tf_op jit(solution)/shard_map/write_out/pallas_call | solution.py:604

commit v5 on v4

--- a/solution.py
+++ b/solution.py
@@ -45,10 +45,11 @@
         wdt1,
         wdt2,
         s0,
-        psend,
-        ptp,
+        hx,
+        wdx,
         ysend,
         yrecv,
+        zdirect,
         accf,
         zsend,
         zrecv,
@@ -69,8 +70,10 @@
         ld,
         ag,
         ag_t,
-        rs_t,
+        hx_s,
+        wd_s,
         rs_y,
+        rs_d,
         rs_z,
         md,
         w_y,
@@ -254,46 +257,64 @@
         return finish
 
     def gated(gate, up):
-        hidden = (gate * jax.nn.sigmoid(gate) * up).astype(BF16)
-        return jnp.concatenate([hidden, jnp.zeros((128 - HID, R), BF16)], axis=0)
+        return (gate * jax.nn.sigmoid(gate) * up).astype(BF16)
 
     def half(phase, hidden, wdt, meanwhile, residual):
-        for k in range(1, NY + 1):
+        hx[phase, 0, 0:HID] = hidden
+        hx[phase, 0, HID:] = jnp.zeros((128 - HID, R), BF16)
+        hx[phase, 1, HID:] = jnp.zeros((128 - HID, R), BF16)
+        units = pl.ds(0, HID)
+        copy_to(
+            hx.at[phase, 0, units],
+            hx.at[phase, 1, units],
+            hx_s.at[phase, 0],
+            hx_s.at[phase, 1],
+            **other,
+        ).start()
+        owe(hx.at[phase, 0, units], hx_s.at[phase, 0])
+        far = [(i, pl.ds(lax.rem(z // G + o, NG) * G, G)) for i, o in enumerate(order[::-1])]
+        got(wdx.at[phase], wd_s.at[phase, 1])
+        got(hx.at[phase, 1, units], hx_s.at[phase, 1])
+        pair_hidden = hx[phase].reshape(256, R)
+        for slot, k in ((2, 2), (0, 1), (1, 3), (None, 4)):
             yy = lax.rem(y + k, NY)
-            w = wdt[1 - t, yy].reshape(NZ * C, 128)
-            psend[phase, k - 1] = dot(w, hidden, 1, 0).astype(BF16).reshape(NZ, C, R)
-            copy_to(
-                psend.at[phase, k - 1],
-                ptp.at[phase, k - 1],
-                rs_t.at[phase, 0],
-                rs_t.at[phase, k],
-                **other,
-            ).start()
-        owe(psend.at[phase], rs_t.at[phase, 0])
-        far = [(i, pl.ds(lax.rem(z // G + o, NG) * G, G)) for i, o in enumerate(order[::-1])]
-        for k in range(1, NY + 1):
-            yy = lax.rem(y + k, NY)
-            w = wdt[t, yy].reshape(NZ * C, 128)
-            mine = dot(w, hidden, 1, 0).reshape(NZ, C, R)
-            got(ptp.at[phase, k - 1], rs_t.at[phase, k])
-            both = mine + ptp[phase, k - 1].astype(F32)
-            if k < NY:
-                ysend[phase, k - 1] = both.astype(BF16)
-                for i, part in far:
+            w = [wdt[t, yy].reshape(NZ * C, 128), wdx[phase, yy].reshape(NZ * C, 128)]
+            both = dot(jnp.concatenate(w, axis=1), pair_hidden, 1, 0).reshape(NZ, C, R)
+            if k == 4:
+                break
+            ysend[phase, slot] = both.astype(BF16)
+            if k == 2:
+
+                def direct(i, c):
+                    kz = lax.rem(far_first(i), NZ)
+                    zz = zpeer(kz)
                     copy_to(
-                        ysend.at[phase, k - 1, part],
-                        yrecv.at[phase, k - 1, part],
-                        rs_y.at[phase, 0],
-                        rs_y.at[phase, 1 + i],
-                        **at_y(yy),
+                        ysend.at[phase, 2, zz],
+                        zdirect.at[phase, kz],
+                        rs_d.at[phase, 0],
+                        rs_d.at[phase, 1],
+                        kv=zz * NY + lax.rem(y + 2, NY),
                     ).start()
+                    return c
+
+                lax.fori_loop(0, NZ, direct, 0)
+                continue
+            for i, part in far:
+                copy_to(
+                    ysend.at[phase, slot, part],
+                    yrecv.at[phase, slot, part],
+                    rs_y.at[phase, 0],
+                    rs_y.at[phase, 1 + i],
+                    **at_y(yy),
+                ).start()
         accf[phase] = both
-        owe(ysend.at[phase], rs_y.at[phase, 0])
+        owe(ysend.at[phase, pl.ds(0, 2)], rs_y.at[phase, 0])
+        owe(ysend.at[phase, 2], rs_d.at[phase, 0])
         for i, part in far:
             got(yrecv.at[phase, :, part], rs_y.at[phase, 1 + i])
             sums = accf[phase, part]
-            for k in range(1, NY):
-                sums = sums + yrecv[phase, k - 1, part].astype(F32)
+            for slot in range(2):
+                sums = sums + yrecv[phase, slot, part].astype(F32)
             accf[phase, part] = sums
             zsend[phase, part] = sums.astype(BF16)
             for j in range(G):
@@ -315,9 +336,18 @@
         meanwhile()
         total = accf[phase, z]
         got(landed, rs_z.at[phase, 1])
-        for k in range(1, NZ):
-            total = total + zrecv[phase, k].astype(F32)
+        got(zdirect.at[phase], rs_d.at[phase, 1])
+        for k in range(NZ):
+            total = total + zdirect[phase, k].astype(F32)
+            if k:
+                total = total + zrecv[phase, k].astype(F32)
         return (residual() + 0.5 * total).astype(BF16)
+
+    def share_down(phase, wdt):
+        copy_to(
+            wdt.at[1 - t], wdx.at[phase], wd_s.at[phase, 0], wd_s.at[phase, 1], **other
+        ).start()
+        owe(wdx.at[phase], wd_s.at[phase, 0])
 
     gat1[z, y, t] = s0[...]
     finish = gather(
@@ -328,6 +358,7 @@
         ag_t.at[0],
     )
     wsh[y] = wall[pl.ds(4 * y, 4)]
+    share_down(0, wdt1)
     finish()
     all_rows = gat1[...].reshape(D, R)
     acc = dot(wgu1[...], all_rows, 1, 0)
@@ -446,6 +477,7 @@
     turn(wdt2, wd2)
     got(wog.at[pl.ds(0, NY - 1)], wo_y.at[1])
     got(mg.at[pl.ds(0, NZ - 1)], mh.at[1])
+    share_down(1, wdt2)
     mgf[...] = mg[...].astype(F32).reshape(NZ * 8, 128)
     heads = []
     for h in range(4):
@@ -564,10 +596,11 @@
             V((2, NY, NZ, C, 128), BF16),
             V((2, NY, NZ, C, 128), BF16),
             V((C, R), BF16),
-            V((2, NY, NZ, C, R), BF16),
-            V((2, NY, NZ, C, R), BF16),
-            V((2, NY - 1, NZ, C, R), BF16),
-            V((2, NY - 1, NZ, C, R), BF16),
+            V((2, 2, 128, R), BF16),
+            V((2, NY, NZ, C, 128), BF16),
+            V((2, 3, NZ, C, R), BF16),
+            V((2, 2, NZ, C, R), BF16),
+            V((2, NZ, C, R), BF16),
             V((2, NZ, C, R), F32),
             V((2, NZ, C, R), BF16),
             V((2, NZ, C, R), BF16),
@@ -588,8 +621,10 @@
             S((19,)),
             S((2, 2 + NY * NG)),
             S((2, 2)),
-            S((2, 1 + NY)),
+            S((2, 2)),
+            S((2, 2)),
             S((2, 1 + NG)),
+            S((2, 2)),
             S((2, 2)),
             S((2,)),
             S((2,)),

time: 92 us -> 90.5 us (0.984)
  Pallas kernels: 91.2 us -> 89.7 us
    pallas_call x1, Pallas kernels: 89.5 us -> 88 us  [body(): pl.pallas_call(functools.partial(kernel, NZ, first_gate.shape[1]), out_sh...]
where the time goes in v5:
time: 90.5 us; the launch traced here: 90.3 us
  Pallas kernels  89.7 us (99%)
    pallas_call x1, Pallas kernels, body(): pl.pallas_call(functools.partial(kernel, NZ, first_gate.shape[1]), out_sh...  88 us

profile of v5, /device:TPU:6, one launch (start us, length us, event | category | flops | bytes accessed | tf_op | source)
XLA Modules:
  0.0 90.3 jit_solution(3417432539308662490)
XLA Ops:
  0.6 88.0 %layer.1 = (bf16[16,128]{1,0:T(8,128)(2,1)}, f32[2,4,64,128]{3,2,1,0:T(8,128)}) custom-call(bf16[16,128]{1,0:T(8,128)(2,1)} %bitcast.18, f32[2,4,64,128]{3,2,1,0:T(8,128)} %refs_1_.1, f32[2,256]{1,0:T(2,128)} %refs_2_.1, f32[1,2048]{1,0:T(1,128)} %bitcast.16, bf16[44,2048]{1,0:T(8,128)(2,1)} %bitcast.11, bf16[44,2048]{1,0:T(8,128)(2,1)} %bitcast.12, ...), custom_call_target="tpu_custom_call" | custom-call | tf_op jit(solution)/shard_map/layer/pallas_call | solution.py:581
  88.6 1.7 %write_out.1 = (bf16[16,128]{1,0:T(8,128)(2,1)}, f32[2,4,64,128]{3,2,1,0:T(8,128)}) custom-call(bf16[16,128]{1,0:T(8,128)(2,1)} %get-tuple-element.6.outT, f32[2,4,64,128]{3,2,1,0:T(8,128)} %get-tuple-element.7.new), custom_call_target="tpu_custom_call" | custom-call | tf_op jit(solution)/shard_map/write_out/pallas_call | solution.py:639

commit v6 on v5

--- a/solution.py
+++ b/solution.py
@@ -210,11 +210,11 @@
     def got(ref, sem):
         copy_to(ref, ref, sem, sem, **other).wait_recv()
 
-    G = max(NZ // 4, 1)
+    G = max(NZ // 8, 1)
     NG = NZ // G
     order = [0] + [(i + 1) // 2 if i % 2 else NG - i // 2 for i in range(1, NG)]
 
-    def gather(slot, most, sem, everything=None, pair_sem=None):
+    def gather(slot, columns, sem, pair_sem):
         mine = slot(z, 1, y)
 
         def send(i, c):
@@ -237,22 +237,20 @@
                         group,
                         group,
                         sem.at[1 + NG],
-                        sem.at[arrival + (j - 1) * NG + i],
+                        sem.at[arrival + i],
                         **at_y(ypeer(j)),
                     ).start()
-                if pair_sem is not None:
-                    copy_to(group, group, pair_sem.at[0], pair_sem.at[1], **other).start()
+                copy_to(group, group, pair_sem.at[0], pair_sem.at[1], **other).start()
             for i in range(NG):
                 q = lax.rem(z // G + order[i], NG)
+                got(columns(0, G, NY - 1), sem.at[arrival + i])
                 for j in (1, 3, 2):
                     group = slot(q * G, G, yfrom(j))
-                    got(group, sem.at[arrival + (j - 1) * NG + i])
-                    if pair_sem is not None:
-                        copy_to(group, group, pair_sem.at[0], pair_sem.at[1], **other).start()
-            owe(most, sem.at[1 + NG])
-            if pair_sem is not None:
-                got(everything, pair_sem.at[1])
-                owe(everything, pair_sem.at[0])
+                    copy_to(group, group, pair_sem.at[0], pair_sem.at[1], **other).start()
+            owe(columns(0, NZ, NY - 1), sem.at[1 + NG])
+            everything = columns(0, NZ, NY)
+            got(everything, pair_sem.at[1])
+            owe(everything, pair_sem.at[0])
 
         return finish
 
@@ -352,9 +350,8 @@
     gat1[z, y, t] = s0[...]
     finish = gather(
         lambda zz, n, yy: gat1.at[pl.ds(zz, n), yy, t],
-        gat1.at[:, pl.ds(0, NY - 1), t],
+        lambda zz, n, m: gat1.at[pl.ds(zz, n), pl.ds(0, m), t],
         ag.at[0],
-        gat1.at[:, :, t],
         ag_t.at[0],
     )
     wsh[y] = wall[pl.ds(4 * y, 4)]
@@ -494,9 +491,8 @@
     gat2[z, y, t] = (trn[2 * y + t] + attention).astype(BF16)
     gather(
         lambda zz, n, yy: gat2.at[pl.ds(zz, n), yy, t],
-        gat2.at[:, pl.ds(0, NY - 1), t],
+        lambda zz, n, m: gat2.at[pl.ds(zz, n), pl.ds(0, m), t],
         ag.at[1],
-        gat2.at[:, :, t],
         ag_t.at[1],
     )()
     all_rows = jnp.concatenate([gat2[i].reshape(R, NY * 2 * C) for i in range(NZ)], axis=1)
@@ -554,7 +550,7 @@
     NZ = lax.axis_size("kv") // NY
     R = 2 * NY * NZ
     D = NY * NZ * 2 * C
-    NG = NZ // max(NZ // 4, 1)
+    NG = NZ // max(NZ // 8, 1)
     V = pltpu.VMEM
     S = pltpu.SemaphoreType.DMA
     arrays = (
@@ -619,7 +615,7 @@
             V((NZ, NY * 2 * C), BF16),
             V((2 * NY, C, R), F32),
             S((19,)),
-            S((2, 2 + NY * NG)),
+            S((2, 2 + 2 * NG)),
             S((2, 2)),
             S((2, 2)),
             S((2, 2)),

time: 90.5 us -> 89.3 us (0.987)
  Pallas kernels: 89.7 us -> 88.4 us
    pallas_call x1, Pallas kernels: 88 us -> 86.8 us  [body(): pl.pallas_call(functools.partial(kernel, NZ, first_gate.shape[1]), out_sh...]
where the time goes in v6:
time: 89.3 us; the launch traced here: 89.1 us
  Pallas kernels  88.4 us (99%)
    pallas_call x1, Pallas kernels, body(): pl.pallas_call(functools.partial(kernel, NZ, first_gate.shape[1]), out_sh...  86.8 us

profile of v6, /device:TPU:6, one launch (start us, length us, event | category | flops | bytes accessed | tf_op | source)
XLA Modules:
  0.0 89.1 jit_solution(12506378967294264936)
XLA Ops:
  0.6 86.8 %layer.1 = (bf16[16,128]{1,0:T(8,128)(2,1)}, f32[2,4,64,128]{3,2,1,0:T(8,128)}) custom-call(bf16[16,128]{1,0:T(8,128)(2,1)} %bitcast.18, f32[2,4,64,128]{3,2,1,0:T(8,128)} %refs_1_.1, f32[2,256]{1,0:T(2,128)} %refs_2_.1, f32[1,2048]{1,0:T(1,128)} %bitcast.16, bf16[44,2048]{1,0:T(8,128)(2,1)} %bitcast.11, bf16[44,2048]{1,0:T(8,128)(2,1)} %bitcast.12, ...), custom_call_target="tpu_custom_call" | custom-call | tf_op jit(solution)/shard_map/layer/pallas_call | solution.py:577
  87.4 1.7 %write_out.1 = (bf16[16,128]{1,0:T(8,128)(2,1)}, f32[2,4,64,128]{3,2,1,0:T(8,128)}) custom-call(bf16[16,128]{1,0:T(8,128)(2,1)} %get-tuple-element.6.outT, f32[2,4,64,128]{3,2,1,0:T(8,128)} %get-tuple-element.7.new), custom_call_target="tpu_custom_call" | custom-call | tf_op jit(solution)/shard_map/write_out/pallas_call | solution.py:635

commit v7 on v6

--- a/solution.py
+++ b/solution.py
@@ -378,7 +378,7 @@
 
     here = midg.at[2 * y + t]
     here[...] = middle
-    for k in range(NY):
+    for k in (2, 1, 3, 0):
         where = at_y(ypeer(k))
         copy_to(here, here, md.at[0], md.at[1], **where, **other).start()
         if k:
@@ -470,11 +470,11 @@
     sends.append(out_copy.wait)
     for i in (15, 16, 17, 18):
         load(i).wait()
+    turn(wdt2, wd2)
     fold(wgu2, wg2, wu2, g2)
-    turn(wdt2, wd2)
+    share_down(1, wdt2)
     got(wog.at[pl.ds(0, NY - 1)], wo_y.at[1])
     got(mg.at[pl.ds(0, NZ - 1)], mh.at[1])
-    share_down(1, wdt2)
     mgf[...] = mg[...].astype(F32).reshape(NZ * 8, 128)
     heads = []
     for h in range(4):

time: 89.3 us -> 89.7 us (level)
  no operation moved by 1% of the time
where the time goes in v7:
time: 89.7 us; the launch traced here: 89.5 us
  Pallas kernels  88.9 us (99%)
    pallas_call x1, Pallas kernels, body(): pl.pallas_call(functools.partial(kernel, NZ, first_gate.shape[1]), out_sh...  87.2 us

profile of v7, /device:TPU:6, one launch (start us, length us, event | category | flops | bytes accessed | tf_op | source)
XLA Modules:
  0.0 89.5 jit_solution(4510198989036013003)
XLA Ops:
  0.6 87.2 %layer.1 = (bf16[16,128]{1,0:T(8,128)(2,1)}, f32[2,4,64,128]{3,2,1,0:T(8,128)}) custom-call(bf16[16,128]{1,0:T(8,128)(2,1)} %bitcast.18, f32[2,4,64,128]{3,2,1,0:T(8,128)} %refs_1_.1, f32[2,256]{1,0:T(2,128)} %refs_2_.1, f32[1,2048]{1,0:T(1,128)} %bitcast.16, bf16[44,2048]{1,0:T(8,128)(2,1)} %bitcast.11, bf16[44,2048]{1,0:T(8,128)(2,1)} %bitcast.12, ...), custom_call_target="tpu_custom_call" | custom-call | tf_op jit(solution)/shard_map/layer/pallas_call | solution.py:577
  87.8 1.7 %write_out.1 = (bf16[16,128]{1,0:T(8,128)(2,1)}, f32[2,4,64,128]{3,2,1,0:T(8,128)}) custom-call(bf16[16,128]{1,0:T(8,128)(2,1)} %get-tuple-element.6.outT, f32[2,4,64,128]{3,2,1,0:T(8,128)} %get-tuple-element.7.new), custom_call_target="tpu_custom_call" | custom-call | tf_op jit(solution)/shard_map/write_out/pallas_call | solution.py:635

commit v8 on v6

--- a/solution.py
+++ b/solution.py
@@ -513,8 +513,10 @@
 
 
 def write_out(outT, new, outT_ref, new_ref, o_v, n_v, sem):
-    parts = new.shape[0]
-    moves = [(outT, o_v, outT_ref)] + [(new.at[i], n_v.at[i], new_ref.at[i]) for i in range(parts)]
+    moves = [(outT, o_v, outT_ref)]
+    for i in range(new.shape[0]):
+        for h in range(new.shape[1]):
+            moves.append((new.at[i, h], n_v.at[i, h], new_ref.at[i, h]))
     ins = [pltpu.make_async_copy(a, v, sem.at[0, i]) for i, (a, v, _) in enumerate(moves)]
     outs = [pltpu.make_async_copy(v, b, sem.at[1, i]) for i, (_, v, b) in enumerate(moves)]
     for c in ins:
@@ -640,7 +642,7 @@
         ),
         in_specs=[pl.BlockSpec(memory_space=pl.ANY)] * 2,
         out_specs=[pl.BlockSpec(memory_space=pl.ANY)] * 2,
-        scratch_shapes=[V(outT.shape, BF16), V(new.shape, F32), S((2, 1 + new.shape[0]))],
+        scratch_shapes=[V(outT.shape, BF16), V(new.shape, F32), S((2, 1 + new.shape[0] * new.shape[1]))],
         name="write_out",
     )(outT, new)
     return outT.T, new

time: 89.3 us -> 89.3 us (level)
  no operation moved by 1% of the time
where the time goes in v8:
time: 89.3 us; the launch traced here: 89.1 us
  Pallas kernels  88.4 us (99%)
    pallas_call x1, Pallas kernels, body(): pl.pallas_call(functools.partial(kernel, NZ, first_gate.shape[1]), out_sh...  86.8 us

profile of v8, /device:TPU:6, one launch (start us, length us, event | category | flops | bytes accessed | tf_op | source)
XLA Modules:
  0.0 89.1 jit_solution(3356265025179054837)
XLA Ops:
  0.6 86.8 %layer.1 = (bf16[16,128]{1,0:T(8,128)(2,1)}, f32[2,4,64,128]{3,2,1,0:T(8,128)}) custom-call(bf16[16,128]{1,0:T(8,128)(2,1)} %bitcast.18, f32[2,4,64,128]{3,2,1,0:T(8,128)} %refs_1_.1, f32[2,256]{1,0:T(2,128)} %refs_2_.1, f32[1,2048]{1,0:T(1,128)} %bitcast.16, bf16[44,2048]{1,0:T(8,128)(2,1)} %bitcast.11, bf16[44,2048]{1,0:T(8,128)(2,1)} %bitcast.12, ...), custom_call_target="tpu_custom_call" | custom-call | tf_op jit(solution)/shard_map/layer/pallas_call | solution.py:579
  87.4 1.6 %write_out.1 = (bf16[16,128]{1,0:T(8,128)(2,1)}, f32[2,4,64,128]{3,2,1,0:T(8,128)}) custom-call(bf16[16,128]{1,0:T(8,128)(2,1)} %get-tuple-element.6.outT, f32[2,4,64,128]{3,2,1,0:T(8,128)} %get-tuple-element.7.new), custom_call_target="tpu_custom_call" | custom-call | tf_op jit(solution)/shard_map/write_out/pallas_call | solution.py:637
